TPU v7x, 512 devices: a whole 4x8x8 slice. The times are simulated.
512 devices in a mesh: fs: 64 (over z, y), tp: 8 (over x, core).
Axes of the slice: x: 4, y: 8, z: 8, core: 2. Of those that a mesh axis runs over, the one named last changes fastest.
Arguments:
- tokens: bfloat16 [24576, 2048], P('fs', 'tp'), may hold values from -6 to 6
- outer_gate: bfloat16 [2048, 2048], P('fs', 'tp'), may hold values from -0.125 to 0.125
- inner_gate: bfloat16 [2048, 2048], P('fs', 'tp'), may hold values from -0.125 to 0.125
- mix_value: bfloat16 [2048, 2048], P('fs', 'tp'), may hold values from -0.125 to 0.125
- mix_taps: bfloat16 [3, 2048], P(None, 'tp'), may hold values from -3 to 3
- mix_out: bfloat16 [2048, 2048], P('tp', 'fs'), may hold values from -0.375 to 0.375
- mix_gain: bfloat16 [2048], P('tp'), may hold values from 0.099609375 to 1.8984375
- ffn_gate: bfloat16 [2048, 3072], P('fs', 'tp'), may hold values from -0.125 to 0.125
- ffn_value: bfloat16 [2048, 3072], P('fs', 'tp'), may hold values from -0.125 to 0.125
- gate_taps: bfloat16 [3, 3072], P(None, 'tp'), may hold values from -3 to 3
- value_taps: bfloat16 [3, 3072], P(None, 'tp'), may hold values from -3 to 3
- ffn_down: bfloat16 [3072, 2048], P('tp', 'fs'), may hold values from -0.3125 to 0.3125
- ffn_gain: bfloat16 [2048], P('tp'), may hold values from 0.099609375 to 1.8984375
Outputs:
- layer_out: bfloat16 [24576, 2048], P('fs', 'tp')
All inputs are finite; a program needn't handle non-finite values.
Results may differ from a plain program's by a relative error of at most 0.015.
Values may be sent and summed in bfloat16 or wider, within the bound.
A program may use at most 64 MiB of HBM per device.

v0:
```python
import jax
import jax.numpy as jnp
from jax import lax
from jax.sharding import PartitionSpec as P

SEQ_LEN = 128


residual_scale = 8.0**0.25
norm_epsilon = 1e-05


def copy_for_each(value, axis):
    copies = jnp.broadcast_to(value, (lax.axis_size(axis), *value.shape))
    return lax.all_to_all(copies, axis, split_axis=0, concat_axis=0, tiled=True)


def taken_together(value, axis):
    everything = copy_for_each(value, axis)
    return jnp.sum(everything, axis=0)


def in_one(arrays, axis):
    ends = [0]
    for a in arrays:
        ends.append(ends[-1] + a.size)
    subtotal = taken_together(jnp.concatenate([a.ravel() for a in arrays]), axis)
    return tuple((subtotal[b:e].reshape(a.shape) for a, b, e in zip(arrays, ends, ends[1:])))


def in_one_piece(arrays, axis, dim, along):
    both = jnp.concatenate(arrays, axis=along)
    filled, at, finished = (lax.all_gather(both, axis, axis=dim, tiled=True), 0, [])
    for a in arrays:
        finished.append(lax.slice_in_dim(filled, at, at + a.shape[along], axis=along))
        at += a.shape[along]
    return tuple(finished)


def laid_out(blocks, dim):
    blocks = jnp.moveaxis(blocks, 0, dim)
    dims = blocks.shape
    return blocks.reshape(*dims[:dim], dims[dim] * dims[dim + 1], *dims[dim + 2 :])


def collect(value, axis, dim):
    return laid_out(copy_for_each(value, axis), dim)


def split_up(value, dim, peers):
    before, after = (value.shape[:dim], value.shape[dim + 1 :])
    return jnp.moveaxis(value.reshape(*before, peers, -1, *after), dim, 0)


def sent_and_summed(value, axis, dim):
    peers = lax.axis_size(axis)
    blocks = lax.all_to_all(split_up(value, dim, peers), axis, 0, 0, tiled=True)
    return jnp.sum(blocks.astype(jnp.float32), axis=0)


def stored(values):
    return lax.optimization_barrier(values.astype(jnp.bfloat16)).astype(jnp.float32)


def shift_rows(values, offset):
    position = jnp.arange(values.shape[0]) % SEQ_LEN
    shifted = jnp.concatenate(
        [jnp.zeros((offset, values.shape[1]), values.dtype), values[:-offset]], axis=0
    )
    return jnp.where((position >= offset)[:, None], shifted, jnp.zeros_like(shifted))


def causal_taps(values, taps):
    weights = taps.astype(jnp.float32)
    return (
        values * weights[2]
        + shift_rows(values, 1) * weights[1]
        + shift_rows(values, 2) * weights[0]
    )


def fold_rows(whole, pieces):
    return tuple((jnp.dot(whole, piece, preferred_element_type=jnp.float32) for piece in pieces))


def norm_shares(prenorm, gain):
    width = prenorm.shape[1] * lax.axis_size("tp")
    row_sums = jnp.sum(prenorm, axis=1)
    row_squares = jnp.sum(prenorm * prenorm, axis=1)
    total, total_squares = in_one((row_sums, row_squares), "tp")
    mean = total / width
    spread = total_squares / width - mean * mean
    scaled = (prenorm - mean[:, None]) * lax.rsqrt(spread[:, None] + norm_epsilon)
    return (scaled * gain.astype(jnp.float32)).astype(jnp.bfloat16)


def body(
    tokens,
    outer_gate,
    inner_gate,
    mix_value,
    mix_taps,
    mix_out,
    mix_gain,
    ffn_gate,
    ffn_value,
    gate_taps,
    value_taps,
    ffn_down,
    ffn_gain,
):
    gate_whole, value_whole = in_one_piece((ffn_gate, ffn_value), "fs", 0, 1)
    whole_tokens = collect(tokens, "tp", 1)
    outer, inner, values = fold_rows(
        whole_tokens, in_one_piece((outer_gate, inner_gate, mix_value), "fs", 0, 1)
    )
    outer, inner, values = (stored(outer), stored(inner), stored(values))
    gated = (outer * causal_taps(inner * values, mix_taps)).astype(jnp.bfloat16)
    mixer_terms = jnp.dot(gated, collect(mix_out, "fs", 1), preferred_element_type=jnp.float32)
    mixer_branch = sent_and_summed(mixer_terms.astype(jnp.bfloat16), "tp", 1)
    first_own = norm_shares(residual_scale * tokens.astype(jnp.float32) + mixer_branch, mix_gain)
    first_whole = collect(first_own, "tp", 1)
    gate_up = jnp.dot(first_whole, gate_whole, preferred_element_type=jnp.float32)
    value_up = jnp.dot(first_whole, value_whole, preferred_element_type=jnp.float32)
    gate_up, value_up = (stored(gate_up), stored(value_up))
    hidden = (
        jax.nn.silu(causal_taps(gate_up, gate_taps)) * causal_taps(value_up, value_taps)
    ).astype(jnp.bfloat16)
    ffn_terms = jnp.dot(
        hidden,
        lax.all_gather(ffn_down, "fs", axis=1, tiled=True),
        preferred_element_type=jnp.float32,
    )
    ffn_branch = sent_and_summed(ffn_terms.astype(jnp.bfloat16), "tp", 1)
    return norm_shares(residual_scale * first_own.astype(jnp.float32) + ffn_branch, ffn_gain)


def solution(mesh):
    placed = (
        P("fs", "tp"),
        P("fs", "tp"),
        P("fs", "tp"),
        P("fs", "tp"),
        P(None, "tp"),
        P("tp", "fs"),
        P("tp"),
        P("fs", "tp"),
        P("fs", "tp"),
        P(None, "tp"),
        P(None, "tp"),
        P("tp", "fs"),
        P("tp"),
    )
    return jax.shard_map(body, mesh=mesh, in_specs=placed, out_specs=P("fs", "tp"), check_vma=False)
```

profile of v0, /device:TPU:1, one launch (start us, length us, event | category | flops | bytes accessed | tf_op | source)
XLA Modules:
  0.0 324.7 jit_solution(7652189762097484057)
XLA Ops:
  6.5 1.4 pad_maximum_fusion
  8.0 1.4 pad_maximum_fusion.1
  9.4 1.1 copy.25
  10.6 29.8 %all_to_all.37 = bf16[8,384,256]{1,2,0:T(8,128)(2,1)S(1)} all-to-all(bf16[8,384,256]{1,2,0:T(8,128)(2,1)S(1)} %broadcast_in_dim.65), channel_id=1, replica_groups=mesh['fs'=64,'tp'=8] {'tp'}, dimensions={0} | all-to-all | bytes 3145728 | tf_op jit(solution)/shard_map/all_to_all | solution.py:15
  40.5 1.1 broadcast_in_dim.68
  41.6 12.7 %all-to-all-start.1 = ((bf16[64,256,32]{1,2,0:T(8,128)(2,1)}), bf16[64,256,32]{1,2,0:T(8,128)(2,1)S(1)}, u32[]{:S(2)}, u32[]{:S(2)}) async-start(bf16[64,256,32]{1,2,0:T(8,128)(2,1)} %broadcast_in_dim.68), calls=%async_computation.1 | async-start | bytes 2097152 | tf_op jit(solution)/shard_map/all_to_all | solution.py:15
  54.3 53.7 %all-gather.4.cloned.1.call-done = bf16[2048,768]{1,0:T(8,128)(2,1)} async-done(((bf16[32,768]{1,0:T(8,128)(2,1)}), bf16[2048,768]{1,0:T(8,128)(2,1)}) %all-gather.4.cloned.1.call-update) | async-done | bytes 3145744 | tf_op jit(solution)/shard_map/all_gather | solution.py:33
  108.0 2.0 fusion.11
  110.0 2.0 fusion.12
  112.0 2.0 fusion.10
  115.1 1.3 copy.42
  116.3 8.6 %all-to-all-start.2 = ((bf16[8,384,256]{2,1,0:T(8,128)(2,1)}), bf16[8,384,256]{2,1,0:T(8,128)(2,1)S(1)}, u32[]{:S(2)}, u32[]{:S(2)}) async-start(bf16[8,384,256]{2,1,0:T(8,128)(2,1)} %bitcast.38), calls=%async_computation.2 | async-start | bytes 3145728 | tf_op jit(solution)/shard_map/all_to_all | solution.py:57
  125.7 19.8 %all-to-all-done.2 = bf16[8,384,256]{2,1,0:T(8,128)(2,1)S(1)} async-done(((bf16[8,384,256]{2,1,0:T(8,128)(2,1)}), bf16[8,384,256]{2,1,0:T(8,128)(2,1)S(1)}, u32[]{:S(2)}, u32[]{:S(2)}) %all-to-all-start.2) | async-done | bytes 1572896 | tf_op jit(solution)/shard_map/all_to_all | solution.py:57
  146.6 4.2 %all-to-all-start.3 = ((f32[8,1,768]{2,1,0:T(1,128)}), f32[8,1,768]{2,1,0:T(1,128)S(1)}, u32[]{:S(2)}, u32[]{:S(2)}) async-start(f32[8,1,768]{2,1,0:T(1,128)} %broadcast_in_dim.69), calls=%async_computation.3 | async-start | bytes 49152 | tf_op jit(solution)/shard_map/all_to_all | solution.py:15
  150.8 4.7 %all-to-all-done.3 = f32[8,1,768]{2,1,0:T(1,128)S(1)} async-done(((f32[8,1,768]{2,1,0:T(1,128)}), f32[8,1,768]{2,1,0:T(1,128)S(1)}, u32[]{:S(2)}, u32[]{:S(2)}) %all-to-all-start.3) | async-done | bytes 24608 | tf_op jit(solution)/shard_map/all_to_all | solution.py:15
  155.9 1.3 broadcast_in_dim.70
  157.2 4.3 %all-to-all-start.4 = ((bf16[8,384,256]{1,2,0:T(8,128)(2,1)}), bf16[8,384,256]{1,2,0:T(8,128)(2,1)S(1)}, u32[]{:S(2)}, u32[]{:S(2)}) async-start(bf16[8,384,256]{1,2,0:T(8,128)(2,1)} %broadcast_in_dim.70), calls=%async_computation.4 | async-start | bytes 3145728 | tf_op jit(solution)/shard_map/all_to_all | solution.py:15
  162.2 30.5 %all-gather.6.cloned.1.call-done = bf16[2048,768]{1,0:T(8,128)(2,1)} async-done(((bf16[32,768]{1,0:T(8,128)(2,1)}), bf16[2048,768]{1,0:T(8,128)(2,1)}) %all-gather.6.cloned.1.call-update) | async-done | bytes 3145744 | tf_op jit(solution)/shard_map/all_gather | solution.py:33
  192.7 2.6 fusion.4
  196.5 78.2 %all-gather.8.cloned.1.call-done = bf16[384,2048]{0,1:T(8,128)(2,1)} async-done(((bf16[384,32]{0,1:T(8,128)(2,1)}), bf16[384,2048]{0,1:T(8,128)(2,1)}) %all-gather.8.cloned.1.call-update) | async-done | bytes 1572880 | tf_op jit(solution)/shard_map/all_gather | solution.py:131
  274.7 2.9 convolution_convert_fusion
  277.7 29.6 %all_to_all.38 = bf16[8,384,256]{2,1,0:T(8,128)(2,1)S(1)} all-to-all(bf16[8,384,256]{2,1,0:T(8,128)(2,1)S(1)} %bitcast.45), channel_id=1, replica_groups=mesh['fs'=64,'tp'=8] {'tp'}, dimensions={0} | all-to-all | bytes 3145728 | tf_op jit(solution)/shard_map/all_to_all | solution.py:57
  308.3 4.3 %all-to-all-start.6 = ((f32[8,1,768]{2,1,0:T(1,128)}), f32[8,1,768]{2,1,0:T(1,128)S(1)}, u32[]{:S(2)}, u32[]{:S(2)}) async-start(f32[8,1,768]{2,1,0:T(1,128)} %broadcast_in_dim.73), calls=%async_computation.6 | async-start | bytes 49152 | tf_op jit(solution)/shard_map/all_to_all | solution.py:15
  312.6 4.7 %all-to-all-done.6 = f32[8,1,768]{2,1,0:T(1,128)S(1)} async-done(((f32[8,1,768]{2,1,0:T(1,128)}), f32[8,1,768]{2,1,0:T(1,128)S(1)}, u32[]{:S(2)}, u32[]{:S(2)}) %all-to-all-start.6) | async-done | bytes 24608 | tf_op jit(solution)/shard_map/all_to_all | solution.py:15
  (67 shorter events, 7.3 us)
Async XLA Ops:
  6.5 101.5 %all-gather.4.cloned.1.call-start = ((), (), s32[]{:S(2)}) async-start(), calls=%async_computation.7 | async-start | bytes 3194880 | tf_op jit(solution)/shard_map/all_gather | solution.py:33
  7.9 184.7 %all-gather.6.cloned.1.call-start = ((), (), s32[]{:S(2)}) async-start(), calls=%async_computation.8 | async-start | bytes 3194880 | tf_op jit(solution)/shard_map/all_gather | solution.py:33
  10.6 29.8 %copy-start.1 = (bf16[256,32]{0,1:T(8,128)(2,1)S(1)}, bf16[256,32]{0,1:T(8,128)(2,1)}, u32[]{:S(2)}) copy-start(bf16[256,32]{0,1:T(8,128)(2,1)} %param.18) | copy-start | bytes 49156
  40.5 13.8 %copy-start.2 = (bf16[3,256]{1,0:T(4,128)(2,1)S(1)}, bf16[3,256]{1,0:T(4,128)(2,1)}, u32[]{:S(2)}) copy-start(bf16[3,256]{1,0:T(4,128)(2,1)} %param.17) | copy-start | bytes 4612
  41.6 72.4 %all-to-all-start.1 = ((bf16[64,256,32]{1,2,0:T(8,128)(2,1)}), bf16[64,256,32]{1,2,0:T(8,128)(2,1)S(1)}, u32[]{:S(2)}, u32[]{:S(2)}) async-start(bf16[64,256,32]{1,2,0:T(8,128)(2,1)} %broadcast_in_dim.68), calls=%async_computation.1 | async-start | bytes 2097152 | tf_op jit(solution)/shard_map/all_to_all | solution.py:15
  54.3 59.7 %copy-start.7 = (pred[384]{0:T(512)(128)(4,1)}, pred[384]{0:T(512)(128)(4,1)S(1)}, u32[]{:S(2)}) copy-start(pred[384]{0:T(512)(128)(4,1)S(1)} %get-tuple-element.22) | copy-start | bytes 1156
  54.3 59.7 %copy-start.9 = (pred[384]{0:T(512)(128)(4,1)}, pred[384]{0:T(512)(128)(4,1)S(1)}, u32[]{:S(2)}) copy-start(pred[384]{0:T(512)(128)(4,1)S(1)} %get-tuple-element.23) | copy-start | bytes 1156
  116.3 29.2 %all-to-all-start.2 = ((bf16[8,384,256]{2,1,0:T(8,128)(2,1)}), bf16[8,384,256]{2,1,0:T(8,128)(2,1)S(1)}, u32[]{:S(2)}, u32[]{:S(2)}) async-start(bf16[8,384,256]{2,1,0:T(8,128)(2,1)} %bitcast.38), calls=%async_computation.2 | async-start | bytes 3145728 | tf_op jit(solution)/shard_map/all_to_all | solution.py:57
  124.9 20.8 %copy-start = (bf16[384,256]{1,0:T(8,128)(2,1)S(1)}, bf16[384,256]{1,0:T(8,128)(2,1)}, u32[]{:S(2)}) copy-start(bf16[384,256]{1,0:T(8,128)(2,1)} %param.13) | copy-start | bytes 589828
  124.9 25.9 %copy-start.12 = (bf16[256]{0:T(256)(128)(2,1)S(1)}, bf16[256]{0:T(256)(128)(2,1)}, u32[]{:S(2)}) copy-start(bf16[256]{0:T(256)(128)(2,1)} %param.19) | copy-start | bytes 1540
  124.9 149.7 %all-gather.8.cloned.1.call-start = ((), (), s32[]{:S(2)}) async-start(), calls=%async_computation.9 | async-start | bytes 1597440 | tf_op jit(solution)/shard_map/all_gather | solution.py:131
  146.6 8.9 %all-to-all-start.3 = ((f32[8,1,768]{2,1,0:T(1,128)}), f32[8,1,768]{2,1,0:T(1,128)S(1)}, u32[]{:S(2)}, u32[]{:S(2)}) async-start(f32[8,1,768]{2,1,0:T(1,128)} %broadcast_in_dim.69), calls=%async_computation.3 | async-start | bytes 49152 | tf_op jit(solution)/shard_map/all_to_all | solution.py:15
  157.2 4.3 %copy-start.3 = (bf16[3,384]{1,0:T(4,128)(2,1)S(1)}, bf16[3,384]{1,0:T(4,128)(2,1)}, u32[]{:S(2)}) copy-start(bf16[3,384]{1,0:T(4,128)(2,1)} %param.22) | copy-start | bytes 6916
  157.2 4.3 %copy-start.4 = (bf16[3,384]{1,0:T(4,128)(2,1)S(1)}, bf16[3,384]{1,0:T(4,128)(2,1)}, u32[]{:S(2)}) copy-start(bf16[3,384]{1,0:T(4,128)(2,1)} %param.23) | copy-start | bytes 6916
  157.2 35.5 %all-to-all-start.4 = ((bf16[8,384,256]{1,2,0:T(8,128)(2,1)}), bf16[8,384,256]{1,2,0:T(8,128)(2,1)S(1)}, u32[]{:S(2)}, u32[]{:S(2)}) async-start(bf16[8,384,256]{1,2,0:T(8,128)(2,1)} %broadcast_in_dim.70), calls=%async_computation.4 | async-start | bytes 3145728 | tf_op jit(solution)/shard_map/all_to_all | solution.py:15
  192.7 2.7 copy-start.11
  196.4 78.3 %copy-start.5 = (f32[384]{0:T(512)S(1)}, f32[384]{0:T(512)}, u32[]{:S(2)}) copy-start(f32[384]{0:T(512)} %get-tuple-element.25) | copy-start | bytes 4612
  196.4 78.3 %copy-start.6 = (f32[384]{0:T(512)S(1)}, f32[384]{0:T(512)}, u32[]{:S(2)}) copy-start(f32[384]{0:T(512)} %get-tuple-element.26) | copy-start | bytes 4612
  196.4 78.3 %copy-start.8 = (pred[384]{0:T(512)(128)(4,1)S(1)}, pred[384]{0:T(512)(128)(4,1)}, u32[]{:S(2)}) copy-start(pred[384]{0:T(512)(128)(4,1)} %copy-done.7) | copy-start | bytes 1156
  196.4 78.3 %copy-start.10 = (pred[384]{0:T(512)(128)(4,1)S(1)}, pred[384]{0:T(512)(128)(4,1)}, u32[]{:S(2)}) copy-start(pred[384]{0:T(512)(128)(4,1)} %copy-done.9) | copy-start | bytes 1156
  307.3 5.3 %copy-start.13 = (bf16[256]{0:T(256)(128)(2,1)S(1)}, bf16[256]{0:T(256)(128)(2,1)}, u32[]{:S(2)}) copy-start(bf16[256]{0:T(256)(128)(2,1)} %param.25) | copy-start | bytes 1540
  308.3 9.0 %all-to-all-start.6 = ((f32[8,1,768]{2,1,0:T(1,128)}), f32[8,1,768]{2,1,0:T(1,128)S(1)}, u32[]{:S(2)}, u32[]{:S(2)}) async-start(f32[8,1,768]{2,1,0:T(1,128)} %broadcast_in_dim.73), calls=%async_computation.6 | async-start | bytes 49152 | tf_op jit(solution)/shard_map/all_to_all | solution.py:15
Sparse Core Ops, SparseCore 0:
  10.3 97.6 all-gather.3
  111.0 81.5 all-gather.5
  195.7 78.9 all-gather.7
where the time goes:
time: 326 us; the launch traced here: 325 us
  waiting for transfers between devices  192 us (59%)
  blocking collectives  59.4 us (18%)
  starting transfers between devices  34.1 us (10%)
  matrix products  13.4 us (4%)
  between operations  13.4 us (4%)
  local copies, waits for them, and re-layouts  7.32 us (2%)
  other arithmetic  4.73 us (1%)
    all_gather x2, waiting for transfers between devices, in_one_piece(): lax.all_gather(both, axis, axis=dim, tiled=True)  84.2 us
    all_gather x1, waiting for transfers between devices, body(): lax.all_gather(ffn_down, 'fs', axis=1, tiled=True)  78.2 us
    all_to_all x1, blocking collectives, copy_for_each(): return lax.all_to_all(copies, axis, split_axis=0, concat_axis=0, tiled=True)  29.8 us
    all_to_all x1, blocking collectives, sent_and_summed(): blocks = lax.all_to_all(split_up(value, dim, peers), axis, 0, 0, tiled=True)  29.6 us
    all_to_all x4, starting transfers between devices, copy_for_each(): return lax.all_to_all(copies, axis, split_axis=0, concat_axis=0, tiled=True)  25.5 us
    all_to_all x1, waiting for transfers between devices, sent_and_summed(): blocks = lax.all_to_all(split_up(value, dim, peers), axis, 0, 0, tiled=True)  19.8 us
    all_to_all x4, waiting for transfers between devices, copy_for_each(): return lax.all_to_all(copies, axis, split_axis=0, concat_axis=0, tiled=True)  9.4 us
    all_to_all x1, starting transfers between devices, sent_and_summed(): blocks = lax.all_to_all(split_up(value, dim, peers), axis, 0, 0, tiled=True)  8.57 us
  transfers between devices with their start and end apart: 8, of which 6 were waited for; matrix products, arithmetic and copies ran while one was open for 6% of the time, Pallas kernels for 0%

commit v1 on v0

v1 whole, which is shorter than its diff:
```python
import functools

import jax
import jax.numpy as jnp
from jax import lax
from jax.experimental import pallas as pl
from jax.experimental.pallas import tpu as pltpu
from jax.sharding import PartitionSpec as P

SEQ_LEN = 128
RING_Z = 8
RING_Y = 8
residual_scale = 8.0**0.25
norm_epsilon = 1e-05
MESH = pl.DeviceIdType.MESH
RIGHT, LEFT = 0, 1
VMEM_LIMIT = 60 * 1024 * 1024
F32 = jnp.float32
BF16 = jnp.bfloat16


def nt_dot(a, b):
    return lax.dot_general(a, b, (((1,), (1,)), ((), ())), preferred_element_type=F32)


def kernel(
    cfg,
    tok_ref,
    og_ref,
    ig_ref,
    mv_ref,
    mtaps_ref,
    mo_ref,
    mgain_ref,
    fg_ref,
    fv_ref,
    gtaps_ref,
    vtaps_ref,
    fd_ref,
    fgain_ref,
    out_ref,
    g1,
    g2,
    g3,
    g4,
    tokw,
    gainw,
    proj,
    gated,
    ppart_m,
    pown_m,
    dbuf_m,
    sbuf_m,
    rbuf_m,
    branchw,
    firstw,
    up,
    hidden,
    ppart_f,
    pown_f,
    dbuf_f,
    sbuf_f,
    rbuf_f,
    ybuf,
    stats,
    mtapf,
    gtapf,
    vtapf,
    wsend,
    wrecv,
    loc_sem,
    tok_send,
    tok_recv,
    gain_send,
    gain_recv,
    d_send,
    d_recv,
    x_send,
    x_recv,
    ag_send,
    ag_recv,
    fw_send,
    st_send,
    st_recv,
):
    Z, Y, TP = cfg
    X = TP // 2
    rows, dl = tok_ref.shape
    kr = og_ref.shape[0]
    h = kr // 2
    fl = fg_ref.shape[1]
    D = TP * dl
    fs = lax.axis_index("fs")
    tp = lax.axis_index("tp")
    z, y = fs // Y, fs % Y
    x, c = tp // 2, tp % 2
    partner = 2 * x + (1 - c)
    gs = (g1, g2, g3, g4)

    def ring_id(axis, step):
        if axis == "y":
            return (z * Y + (y + step + Y) % Y, tp)
        return (((z + step + Z) % Z) * Y + y, tp)

    def block(ref, b):
        return ref.at[:, pl.ds(pl.multiple_of(b * dl, dl), dl)]

    local = []

    def place(src, dst):
        copy = pltpu.make_async_copy(src, dst, loc_sem.at[len(local)])
        copy.start()
        local.append(copy)

    for i, ref in enumerate((og_ref, ig_ref, mv_ref)):
        for half in range(2):
            place(ref.at[pl.ds(half * h, h)], g1.at[z, y, half, :, pl.ds(i * dl, dl)])
    for i, ref in enumerate((fg_ref, fv_ref)):
        for half in range(2):
            place(ref.at[pl.ds(half * h, h)], g3.at[z, y, half, :, pl.ds(i * fl, fl)])
    place(tok_ref, block(tokw, tp))

    barrier = pltpu.get_barrier_semaphore()
    for axis in ("y", "z"):
        for step in (1, -1):
            pl.semaphore_signal(barrier, inc=1, device_id=ring_id(axis, step), device_id_type=MESH)
    for d in range(1, TP):
        pl.semaphore_signal(barrier, inc=1, device_id=(fs, (tp + d) % TP), device_id_type=MESH)

    eye = (
        lax.broadcasted_iota(jnp.int32, (kr, kr), 0) == lax.broadcasted_iota(jnp.int32, (kr, kr), 1)
    ).astype(BF16)
    for g, ref in ((g2, mo_ref), (g4, fd_ref)):
        turned = nt_dot(eye, ref[...]).astype(BF16)
        g[z, y, 0] = turned[:h]
        g[z, y, 1] = turned[h:]
    gainw[:, pl.ds(pl.multiple_of(tp * dl, dl), dl)] = jnp.broadcast_to(mgain_ref[...].astype(F32), (8, dl))
    mtapf[...] = mtaps_ref[...].astype(F32)
    gtapf[...] = gtaps_ref[...].astype(F32)
    vtapf[...] = vtaps_ref[...].astype(F32)
    for copy in local:
        copy.wait()
    pl.semaphore_wait(barrier, 4 + TP - 1)

    def piece(w, colour, phase, origin, half):
        g = gs[w]
        cols = g.shape[-1]
        cut = (cols // 128 + 1) // 2 * 128
        if phase == 0:
            lead = (z, origin, 0) if colour == 0 else (origin, y, 1)
            if half is None:
                return g.at[lead]
            span = pl.ds(0, cut) if half == 0 else pl.ds(cut, cols - cut)
            return g.at[(*lead, slice(None), span)]
        across = Y if colour == 0 else Z
        span = pl.ds(0, across) if half is None else pl.ds(half * (across // 2), across // 2)
        return g.at[origin, span, 0] if colour == 0 else g.at[span, origin, 1]

    def weight_copy(w, colour, phase, way, step, incoming=False):
        along_y = (colour == 0) == (phase == 0)
        axis, n, me = ("y", Y, y) if along_y else ("z", Z, z)
        last = step == n // 2 - 1
        half = way if last else None
        shift = -step if way == RIGHT else step
        if incoming:
            shift = shift - 1 if way == RIGHT else shift + 1
        origin = (me + shift + n) % n
        ref = piece(w, colour, phase, origin, half)
        at = (((w * 2 + colour) * 2 + phase) * 2 + way) * 4 + step
        return pltpu.make_async_remote_copy(
            src_ref=ref,
            dst_ref=ref,
            send_sem=wsend.at[at],
            recv_sem=wrecv.at[at],
            device_id=ring_id(axis, 1 if way == RIGHT else -1),
            device_id_type=MESH,
        )

    sent = []

    def steps_of(colour, phase):
        return (Y if (colour == 0) == (phase == 0) else Z) // 2

    def send_weights(w, phase, step):
        for colour in range(2):
            if step < steps_of(colour, phase):
                for way in (RIGHT, LEFT):
                    copy = weight_copy(w, colour, phase, way, step)
                    copy.start()
                    sent.append(copy)

    def pass_on(w, phase, step):
        for colour in range(2):
            for way in (RIGHT, LEFT):
                if step < steps_of(colour, phase):
                    weight_copy(w, colour, phase, way, step, incoming=True).wait_recv()
                if step + 1 < steps_of(colour, phase):
                    copy = weight_copy(w, colour, phase, way, step + 1)
                    copy.start()
                    sent.append(copy)

    def to_tp(src, dst, send_sem, recv_sem, peer):
        return pltpu.make_async_remote_copy(
            src_ref=src, dst_ref=dst, send_sem=send_sem, recv_sem=recv_sem, device_id=(fs, peer), device_id_type=MESH
        )

    most = max(Y, Z) // 2
    send_weights(0, 0, 0)
    send_weights(1, 0, 0)
    for d in range(1, TP):
        peer = (tp + d) % TP
        mine = block(tokw, tp)
        copy = to_tp(mine, mine, tok_send.at[d], tok_recv.at[d], peer)
        copy.start()
        sent.append(copy)
        mine = block(gainw, tp)
        copy = to_tp(mine, mine, gain_send.at[d], gain_recv.at[d], peer)
        copy.start()
        sent.append(copy)
    send_weights(2, 0, 0)
    send_weights(3, 0, 0)
    for step in range(most):
        for w in range(4):
            pass_on(w, 0, step)
            if step == most - 1 and w < 2:
                send_weights(w, 1, 0)
    for step in range(most):
        for w in range(2):
            if step == most - 1 and w == 0:
                send_weights(2, 1, 0)
                send_weights(3, 1, 0)
            pass_on(w, 1, step)
    for d in range(1, TP):
        peer = (tp - d + TP) % TP
        theirs = block(tokw, peer)
        to_tp(theirs, theirs, tok_send.at[d], tok_recv.at[d], peer).wait_recv()
        theirs = block(gainw, peer)
        to_tp(theirs, theirs, gain_send.at[d], gain_recv.at[d], peer).wait_recv()

    def taps_of(v, tap_ref, cols):
        at = lax.broadcasted_iota(jnp.int32, v.shape, 0)
        one = jnp.where(at >= 1, pltpu.roll(v, 1, 0), 0.0)
        two = jnp.where(at >= 2, pltpu.roll(v, 2, 0), 0.0)
        return v * tap_ref[2:3, cols] + one * tap_ref[1:2, cols] + two * tap_ref[0:1, cols]

    n_seq = rows // SEQ_LEN

    def tiles(cols, body):
        across = cols // 128

        def one(i, carry):
            r = pl.ds(pl.multiple_of((i // across) * SEQ_LEN, SEQ_LEN), SEQ_LEN)
            body(r, pl.multiple_of((i % across) * 128, 128))
            return carry

        lax.fori_loop(0, n_seq * across, one, 0)

    def whole_rows(g, first_col, cols):
        return g[:, :, :, :, pl.ds(first_col, cols)].reshape(D, cols)

    def project(left, g, target):
        def one(n, carry):
            at = pl.multiple_of(n * 256, 256)
            target[:, pl.ds(at, 256)] = jnp.dot(
                left[...], whole_rows(g, at, 256), preferred_element_type=F32
            ).astype(BF16)
            return carry

        lax.fori_loop(0, g.shape[-1] // 256, one, 0)

    def reduce_start(slot, left, g, ppart, pown, dbuf):
        def theirs(j, carry):
            rhs = g[2 * j + 1 - c].reshape(dl, g.shape[-1])
            ppart[j] = nt_dot(left[...], rhs).astype(BF16)
            to_tp(ppart.at[j], dbuf.at[j], d_send.at[slot, j], d_recv.at[slot, j], partner).start()
            return carry

        lax.fori_loop(0, X, theirs, 0)

        def ours(j, carry):
            rhs = g[2 * j + c].reshape(dl, g.shape[-1])
            pown[j] = nt_dot(left[...], rhs).astype(BF16)
            return carry

        lax.fori_loop(0, X, ours, 0)

    def d_wait(slot, j, ppart, dbuf):
        to_tp(ppart.at[j], dbuf.at[j], d_send.at[slot, j], d_recv.at[slot, j], partner).wait()

    away = [d for d in (X // 2, *range(1, X)) if d > 0]
    away = list(dict.fromkeys(away))

    def reduce_cross(slot, ppart, pown, dbuf, sbuf, rbuf):
        for d in away:
            j = (x + d) % X
            d_wait(slot, j, ppart, dbuf)
            sbuf[d] = (pown[j].astype(F32) + dbuf[j].astype(F32)).astype(BF16)
            copy = to_tp(sbuf.at[d], rbuf.at[d], x_send.at[slot, d], x_recv.at[slot, d], 2 * j + c)
            copy.start()
            sent.append(copy)
        d_wait(slot, x, ppart, dbuf)

    def reduce_end(slot, pown, dbuf, sbuf, rbuf):
        for d in away:
            to_tp(sbuf.at[d], rbuf.at[d], x_send.at[slot, d], x_recv.at[slot, d], 2 * ((x - d + X) % X) + c).wait_recv()

        def total(r):
            acc = pown[x, r].astype(F32) + dbuf[x, r].astype(F32)
            for d in away:
                acc = acc + rbuf[d, r].astype(F32)
            return acc

        return total

    project(tokw, g1, proj)

    def mix(r, at):
        cols = pl.ds(at, 128)
        outer = proj[r, cols].astype(F32)
        inner = proj[r, pl.ds(pl.multiple_of(dl + at, 128), 128)].astype(F32)
        value = proj[r, pl.ds(pl.multiple_of(2 * dl + at, 128), 128)].astype(F32)
        gated[r, cols] = (outer * taps_of(inner * value, mtapf, cols)).astype(BF16)

    tiles(dl, mix)
    reduce_start(0, gated, g2, ppart_m, pown_m, dbuf_m)
    reduce_cross(0, ppart_m, pown_m, dbuf_m, sbuf_m, rbuf_m)
    for step in range(min(2, most - 1)):
        for w in (2, 3):
            pass_on(w, 1, step)
    total = reduce_end(0, pown_m, dbuf_m, sbuf_m, rbuf_m)
    own_cols = pl.ds(pl.multiple_of(tp * dl, dl), dl)
    for s in range(n_seq):
        r = pl.ds(s * SEQ_LEN, SEQ_LEN)
        branchw[r, own_cols] = total(r).astype(BF16)
    mine = block(branchw, tp)
    for d in away:
        copy = to_tp(mine, mine, ag_send.at[d], ag_recv.at[tp], 2 * ((x + d) % X) + c)
        copy.start()
        sent.append(copy)
    copy = to_tp(mine, mine, ag_send.at[0], ag_recv.at[tp], partner)
    copy.start()
    sent.append(copy)
    for step in range(2, most - 1):
        for w in (2, 3):
            pass_on(w, 1, step)
    for d in away:
        b = 2 * ((x - d + X) % X) + c
        theirs = block(branchw, b)
        to_tp(theirs, theirs, ag_send.at[d], ag_recv.at[b], b).wait_recv()
        copy = to_tp(theirs, theirs, fw_send.at[d], ag_recv.at[b], partner)
        copy.start()
        sent.append(copy)
    for d in [0, *away]:
        b = 2 * ((x - d + X) % X) + 1 - c
        theirs = block(branchw, b)
        to_tp(theirs, theirs, ag_send.at[d], ag_recv.at[b], partner).wait_recv()

    def norm_first(i, carry):
        r = pl.ds(pl.multiple_of(i * 16, 16), 16)
        v = residual_scale * tokw[r, :].astype(F32) + branchw[r, :].astype(F32)
        mean = jnp.sum(v, axis=1, keepdims=True) * (1.0 / D)
        v = v - mean
        spread = jnp.sum(v * v, axis=1, keepdims=True) * (1.0 / D)
        firstw[r, :] = (v * lax.rsqrt(spread + norm_epsilon) * gainw[0:1, :]).astype(BF16)
        return carry

    lax.fori_loop(0, rows // 16, norm_first, 0)

    pass_on(2, 1, most - 1)
    project(firstw, g3, up)

    def gate(r, at):
        cols = pl.ds(at, 128)
        left = taps_of(up[r, cols].astype(F32), gtapf, cols)
        right = taps_of(up[r, pl.ds(pl.multiple_of(fl + at, 128), 128)].astype(F32), vtapf, cols)
        hidden[r, cols] = (left / (1.0 + jnp.exp(-left)) * right).astype(BF16)

    tiles(fl, gate)
    pass_on(3, 1, most - 1)
    reduce_start(1, hidden, g4, ppart_f, pown_f, dbuf_f)
    reduce_cross(1, ppart_f, pown_f, dbuf_f, sbuf_f, rbuf_f)
    total = reduce_end(1, pown_f, dbuf_f, sbuf_f, rbuf_f)
    lane = lax.broadcasted_iota(jnp.int32, (SEQ_LEN, 128), 1)
    for s in range(n_seq):
        r = pl.ds(s * SEQ_LEN, SEQ_LEN)
        v = residual_scale * firstw[r, own_cols].astype(F32) + total(r)
        ybuf[r, :] = v
        mean = jnp.sum(v, axis=1, keepdims=True) * (1.0 / dl)
        v = v - mean
        square = jnp.sum(v * v, axis=1, keepdims=True)
        both = jnp.where(lane == 0, mean, jnp.where(lane == 1, square, 0.0))
        stats[tp, :, s * SEQ_LEN : (s + 1) * SEQ_LEN] = both.T[:8]
    for d in range(1, TP):
        copy = to_tp(stats.at[tp], stats.at[tp], st_send.at[d], st_recv.at[d], (tp + d) % TP)
        copy.start()
        sent.append(copy)
    for d in range(1, TP):
        b = (tp - d + TP) % TP
        to_tp(stats.at[b], stats.at[b], st_send.at[d], st_recv.at[d], b).wait_recv()
    row8 = lax.broadcasted_iota(jnp.int32, (128, SEQ_LEN), 0)
    for s in range(n_seq):
        r = pl.ds(s * SEQ_LEN, SEQ_LEN)
        theirs = stats[:, :, s * SEQ_LEN : (s + 1) * SEQ_LEN]
        means, squares = theirs[:, 0], theirs[:, 1]
        mean = jnp.sum(means, axis=0, keepdims=True) * (1.0 / TP)
        off = means - mean
        spread = (jnp.sum(squares, axis=0, keepdims=True) + dl * jnp.sum(off * off, axis=0, keepdims=True)) * (1.0 / D)
        scale = lax.rsqrt(spread + norm_epsilon)
        both = jnp.where(row8 == 0, mean, jnp.where(row8 == 1, scale, 0.0)).T
        v = (ybuf[r, :] - both[:, 0:1]) * both[:, 1:2]
        out_ref[r, :] = (v * fgain_ref[...].astype(F32)).astype(BF16)
    for copy in sent:
        copy.wait_send()


def layer(cfg, tokens, outer_gate, inner_gate, mix_value, mix_taps, mix_out, mix_gain, ffn_gate, ffn_value, gate_taps, value_taps, ffn_down, ffn_gain):
    Z, Y, TP = cfg
    X = TP // 2
    rows, dl = tokens.shape
    kr = outer_gate.shape[0]
    h = kr // 2
    fl = ffn_gate.shape[1]
    D = TP * dl
    ring = 4 * 2 * 2 * 2 * 4
    vmem = pl.BlockSpec(memory_space=pltpu.VMEM)
    hbm = pl.BlockSpec(memory_space=pl.ANY)
    dma = pltpu.SemaphoreType.DMA
    blocks = [
        pltpu.VMEM((X, rows, dl), BF16),
        pltpu.VMEM((X, rows, dl), BF16),
        pltpu.VMEM((X, rows, dl), BF16),
        pltpu.VMEM((X, rows, dl), BF16),
        pltpu.VMEM((X, rows, dl), BF16),
    ]
    return pl.pallas_call(
        functools.partial(kernel, cfg),
        out_shape=jax.ShapeDtypeStruct((rows, dl), BF16),
        in_specs=[hbm, hbm, hbm, hbm, vmem, vmem, vmem, hbm, hbm, vmem, vmem, vmem, vmem],
        out_specs=vmem,
        scratch_shapes=[
            pltpu.VMEM((Z, Y, 2, h, 3 * dl), BF16),
            pltpu.VMEM((Z, Y, 2, h, dl), BF16),
            pltpu.VMEM((Z, Y, 2, h, 2 * fl), BF16),
            pltpu.VMEM((Z, Y, 2, h, fl), BF16),
            pltpu.VMEM((rows, D), BF16),
            pltpu.VMEM((8, D), F32),
            pltpu.VMEM((rows, 3 * dl), BF16),
            pltpu.VMEM((rows, dl), BF16),
            *blocks,
            pltpu.VMEM((rows, D), BF16),
            pltpu.VMEM((rows, D), BF16),
            pltpu.VMEM((rows, 2 * fl), BF16),
            pltpu.VMEM((rows, fl), BF16),
            *blocks,
            pltpu.VMEM((rows, dl), F32),
            pltpu.VMEM((TP, 8, rows), F32),
            pltpu.VMEM((3, dl), F32),
            pltpu.VMEM((3, fl), F32),
            pltpu.VMEM((3, fl), F32),
            dma((ring,)),
            dma((ring,)),
            dma((11,)),
            dma((TP,)),
            dma((TP,)),
            dma((TP,)),
            dma((TP,)),
            dma((2, X)),
            dma((2, X)),
            dma((2, X)),
            dma((2, X)),
            dma((X,)),
            dma((TP,)),
            dma((X,)),
            dma((TP,)),
            dma((TP,)),
        ],
        compiler_params=pltpu.CompilerParams(
            collective_id=0, has_side_effects=True, vmem_limit_bytes=VMEM_LIMIT
        ),
    )(
        tokens,
        outer_gate,
        inner_gate,
        mix_value,
        mix_taps,
        mix_out,
        mix_gain.reshape(1, dl),
        ffn_gate,
        ffn_value,
        gate_taps,
        value_taps,
        ffn_down,
        ffn_gain.reshape(1, dl),
    )


def solution(mesh):
    placed = (
        P("fs", "tp"),
        P("fs", "tp"),
        P("fs", "tp"),
        P("fs", "tp"),
        P(None, "tp"),
        P("tp", "fs"),
        P("tp"),
        P("fs", "tp"),
        P("fs", "tp"),
        P(None, "tp"),
        P(None, "tp"),
        P("tp", "fs"),
        P("tp"),
    )
    cfg = (RING_Z, RING_Y, mesh.shape["tp"])
    return jax.shard_map(
        functools.partial(layer, cfg), mesh=mesh, in_specs=placed, out_specs=P("fs", "tp"), check_vma=False
    )
```

time: 326 us -> 117 us (0.36)
  waiting for transfers between devices: 192 us -> 0 us
  Pallas kernels: 0 us -> 111 us
  blocking collectives: 59.4 us -> 0 us
  starting transfers between devices: 34.1 us -> 0 us
  matrix products: 13.4 us -> 0 us
  between operations: 13.4 us -> 0.01 us
  other arithmetic: 4.73 us -> 0 us
    all_gather x3 -> x0, waiting for transfers between devices: 162 us -> none  [the longest x2 84.2 us: in_one_piece(): lax.all_gather(both, axis, axis=dim, tiled=True)]
    pallas_call x0 -> x1, Pallas kernels: none -> 111 us  [layer(): pl.pallas_call(functools.partial(kernel, cfg), out_shape=jax.ShapeDtypeSt...]
    all_to_all x2 -> x0, blocking collectives: 59.4 us -> none  [the longest x1 29.8 us: copy_for_each(): return lax.all_to_all(copies, axis, split_axis=0, concat_axis=0, tiled=True)]
    all_to_all x5 -> x0, starting transfers between devices: 34.1 us -> none  [the longest x4 25.5 us: copy_for_each(): return lax.all_to_all(copies, axis, split_axis=0, concat_axis=0, tiled=True)]
    all_to_all x5 -> x0, waiting for transfers between devices: 29.2 us -> none  [the longest x1 19.8 us: sent_and_summed(): blocks = lax.all_to_all(split_up(value, dim, peers), axis, 0, 0, tiled=True)]
    dot_general x7 -> x0, matrix products: 13.4 us -> none  [the longest x3 5.89 us: fold_rows(): jnp.dot(whole, piece, preferred_element_type=jnp.float32)]
    broadcast_in_dim x5 -> x0, local copies, waits for them, and re-layouts: 3.83 us -> none  [copy_for_each(): copies = jnp.broadcast_to(value, (lax.axis_size(axis), *value.shape))]
  transfers between devices with their start and end apart: 8 -> 0, of which waited for: 6 -> 0; matrix products, arithmetic and copies ran while one was open for 6% -> 0% of each run, Pallas kernels for 0% -> 0%
where the time goes in v1:
time: 117 us; the launch traced here: 116 us
  Pallas kernels  111 us (95%)
  local copies, waits for them, and re-layouts  5.66 us (5%)
    pallas_call x1, Pallas kernels, layer(): pl.pallas_call(functools.partial(kernel, cfg), out_shape=jax.ShapeDtypeSt...  111 us
    unnamed x7, local copies, waits for them, and re-layouts  3.82 us

profile of v1, /device:TPU:1, one launch (start us, length us, event | category | flops | bytes accessed | tf_op | source)
XLA Modules:
  0.0 116.4 jit_solution(9683193466530680628)
XLA Ops:
  0.0 0.0 copy-start.1
  0.0 1.2 %reshape.6.mgain_ref = bf16[1,256]{1,0:T(2,128)(2,1)} reshape(bf16[256]{0:T(256)(128)(2,1)} %param.19) | data formatting | bytes 1024 | tf_op jit(solution)/shard_map/reshape | solution.py:487
  1.2 0.0 copy-done.1
  1.3 0.6 reshape.7.fgain_ref
  1.8 0.0 copy-start
  1.8 1.4 %copy.14.mo_ref = bf16[256,32]{1,0:T(8,128)(2,1)} copy(bf16[256,32]{0,1:T(8,128)(2,1)} %param.18) | data formatting | bytes 32768 | tf_op args[5]
  3.3 0.0 copy-done
  3.3 0.7 copy.15.fd_ref
  4.0 110.8 %shard_map.127 = bf16[384,256]{1,0:T(8,128)(2,1)} custom-call(bf16[384,256]{1,0:T(8,128)(2,1)} %tok_ref.1, bf16[32,256]{1,0:T(8,128)(2,1)} %og_ref.1, bf16[32,256]{1,0:T(8,128)(2,1)} %ig_ref.1, bf16[32,256]{1,0:T(8,128)(2,1)} %mv_ref.1, bf16[3,256]{1,0:T(4,128)(2,1)} %mtaps_ref.1, bf16[256,32]{1,0:T(8,128)(2,1)} %copy.14.mo_ref, ...), custom_call_target="tpu_custom_call" | custom-call | tf_op jit(solution)/shard_map/pallas_call | solution.py:435
  114.8 1.6 %copy.17 = bf16[384,256]{1,0:T(8,128)(2,1)} copy(bf16[384,256]{1,0:T(8,128)(2,1)} %shard_map.127) | data formatting | bytes 393216
Async XLA Ops:
  0.0 1.3 %copy-start.1 = (bf16[256]{0:T(256)(128)(2,1)S(1)}, bf16[256]{0:T(256)(128)(2,1)}, u32[]{:S(2)}) copy-start(bf16[256]{0:T(256)(128)(2,1)} %param.25) | copy-start | bytes 1540
  1.8 1.5 %copy-start = (bf16[384,32]{0,1:T(8,128)(2,1)S(1)}, bf16[384,32]{0,1:T(8,128)(2,1)}, u32[]{:S(2)}) copy-start(bf16[384,32]{0,1:T(8,128)(2,1)} %param.24) | copy-start | bytes 73732

commit v2 on v0

v2 whole, which is shorter than its diff:
```python
import functools

import jax
import jax.numpy as jnp
from jax import lax
from jax.experimental import pallas as pl
from jax.experimental.pallas import tpu as pltpu
from jax.sharding import PartitionSpec as P

SEQ_LEN = 128
RING_Z = 8
RING_Y = 8
residual_scale = 8.0**0.25
norm_epsilon = 1e-05
MESH = pl.DeviceIdType.MESH
RIGHT, LEFT = 0, 1
LATE = 2
LATE_AT = {
    2: ("mixer", 2),
    3: ("gather_start", 0),
    4: ("gather_start", 1),
    5: ("gather_share", 0),
    6: ("gather_share", 1),
    7: ("gather_share", 2),
    8: None,
}
VMEM_LIMIT = 60 * 1024 * 1024
F32 = jnp.float32
BF16 = jnp.bfloat16


def nt_dot(a, b):
    return lax.dot_general(a, b, (((1,), (1,)), ((), ())), preferred_element_type=F32)


def kernel(
    cfg,
    tok_ref,
    og_ref,
    ig_ref,
    mv_ref,
    mtaps_ref,
    mo_ref,
    mgain_ref,
    fg_ref,
    fv_ref,
    gtaps_ref,
    vtaps_ref,
    fd_ref,
    fgain_ref,
    out_ref,
    g12,
    g34,
    tokw,
    gainw,
    branchw,
    firstw,
    normed,
    proj,
    gated,
    up,
    hidden,
    ppart_m,
    pown_m,
    dbuf_m,
    sbuf_m,
    rbuf_m,
    ppart_f,
    pown_f,
    dbuf_f,
    sbuf_f,
    rbuf_f,
    ybuf,
    stats,
    mtapf,
    gtapf,
    vtapf,
    wrecv,
    wsend,
    loc_sem,
    tok_sem,
    gain_sem,
    dsend,
    drecv,
    xsend,
    xrecv,
    agx_send,
    agx_recv,
    agd_send,
    agd_recv,
    st_send,
    st_recv,
):
    Z, Y, TP = cfg
    X = TP // 2
    rows, dl = tok_ref.shape
    kr = og_ref.shape[0]
    h = kr // 2
    fl = fg_ref.shape[1]
    D = TP * dl
    n_seq = rows // SEQ_LEN
    fs = lax.axis_index("fs")
    tp = lax.axis_index("tp")
    z, y = fs // Y, fs % Y
    x, c = tp // 2, tp % 2
    partner = 2 * x + (1 - c)
    groups = (g12, g34)
    away = list(dict.fromkeys([X // 2, *range(1, X)]))

    def ring_id(axis, step):
        if axis == "y":
            return (z * Y + (y + step + Y) % Y, tp)
        return (((z + step + Z) % Z) * Y + y, tp)

    def span(at, size):
        return pl.ds(pl.multiple_of(at, size), size)

    def remote(src, dst, send_sem, recv_sem, to):
        return pltpu.make_async_remote_copy(
            src_ref=src, dst_ref=dst, send_sem=send_sem, recv_sem=recv_sem, device_id=to, device_id_type=MESH
        )

    def await_recv(box, sem):
        remote(box, box, sem, sem, (fs, partner)).wait_recv()

    def await_send(box, sem):
        remote(box, box, sem, sem, (fs, partner)).wait_send()

    barrier = pltpu.get_barrier_semaphore()
    for axis in ("y", "z"):
        for step in (1, -1):
            pl.semaphore_signal(barrier, inc=1, device_id=ring_id(axis, step), device_id_type=MESH)
    for d in range(1, TP):
        pl.semaphore_signal(barrier, inc=1, device_id=(fs, (tp + d) % TP), device_id_type=MESH)

    def place(g, refs, sem):
        at = 0
        for ref in refs:
            cols = ref.shape[1]
            for half in range(2):
                pltpu.make_async_copy(
                    ref.at[pl.ds(half * h, h)], g.at[z, y, half, :, pl.ds(at, cols)], sem
                ).start()
            at += cols

    own_tokens = pltpu.make_async_copy(tok_ref, tokw.at[:, span(tp * dl, dl)], loc_sem.at[2])
    place(g12, (og_ref, ig_ref, mv_ref, mo_ref), loc_sem.at[0])
    own_tokens.start()
    place(g34, (fg_ref, fv_ref, fd_ref), loc_sem.at[1])
    gainw[:, span(tp * dl, dl)] = jnp.broadcast_to(mgain_ref[...].astype(F32).reshape(1, dl), (8, dl))
    mtapf[...] = mtaps_ref[...].astype(F32)
    gtapf[...] = gtaps_ref[...].astype(F32)
    vtapf[...] = vtaps_ref[...].astype(F32)
    for i, g in enumerate(groups):
        pltpu.make_async_copy(g.at[z, y], g.at[z, y], loc_sem.at[i]).wait()
    own_tokens.wait()
    with jax.named_scope("greet"):
        pl.semaphore_wait(barrier, 4 + TP - 1)

    def piece(w, colour, one, two):
        return groups[w].at[two, one, 0] if colour == 0 else groups[w].at[one, two, 1]

    def rings(colour):
        return (("y", Y, y), ("z", Z, z)) if colour == 0 else (("z", Z, z), ("y", Y, y))

    def recv_sem(w, colour, kind, step):
        return wrecv.at[((w * 2 + colour) * 6 + kind) * 4 + step]

    def send_first(w, colour, step):
        (axis, n, me), (_, _, other) = rings(colour)
        for way in (RIGHT, LEFT):
            if step == n // 2 - 1 and way != w % 2:
                continue
            origin = (me - step + n) % n if way == RIGHT else (me + step) % n
            ref = piece(w, colour, origin, other)
            remote(
                ref, ref, wsend.at[2 * w], recv_sem(w, colour, 5, step), ring_id(axis, 1 if way == RIGHT else -1)
            ).start()

    def first_count(colour, step):
        return 1 if step == rings(colour)[0][1] // 2 - 1 else 2

    def members(n, g):
        return [0] if g == 0 else [g] if g == n // 2 else [g, -g]

    def halves(n, g):
        return ([0], []) if g == 0 else ([], [g]) if g == n // 2 else ([g], [-g])

    def send_second(w, colour, g, step):
        (_, n1, me1), (axis, n2, me2) = rings(colour)
        for way in (RIGHT, LEFT):
            at = members(n1, g) if step < n2 // 2 - 1 else halves(n1, g)[way]
            origin = (me2 - step + n2) % n2 if way == RIGHT else (me2 + step) % n2
            for m in at:
                ref = piece(w, colour, (me1 + m + n1) % n1, origin)
                remote(
                    ref, ref, wsend.at[2 * w + 1], recv_sem(w, colour, g, step), ring_id(axis, 1 if way == RIGHT else -1)
                ).start()

    def second_count(colour, g, step):
        n1, n2 = rings(colour)[0][1], rings(colour)[1][1]
        if step < n2 // 2 - 1:
            return 2 * len(members(n1, g))
        return sum(len(part) for part in halves(n1, g))

    def await_pieces(w, count, sem):
        g = groups[w]
        await_recv(g.at[0, 0, 0] if count == 1 else g.at[pl.ds(0, count), 0, 0], sem)

    def begin(w):
        for colour in range(2):
            send_first(w, colour, 0)
        for colour in range(2):
            send_second(w, colour, 0, 0)

    def tick(w, k):
        for colour in range(2):
            n1 = rings(colour)[0][1]
            if 0 <= k < n1 // 2:
                await_pieces(w, first_count(colour, k), recv_sem(w, colour, 5, k))
                if k + 1 < n1 // 2:
                    send_first(w, colour, k + 1)
                send_second(w, colour, k + 1, 0)
        for step in range(max(Y, Z) // 2):
            for colour in range(2):
                n1, n2 = rings(colour)[0][1], rings(colour)[1][1]
                g = k - step
                if 0 <= g <= n1 // 2 and step < n2 // 2:
                    await_pieces(w, second_count(colour, g, step), recv_sem(w, colour, g, step))
                    if step + 1 < n2 // 2:
                        send_second(w, colour, g, step + 1)

    ticks = (Y + Z) // 2

    def late_tick(k):
        with jax.named_scope(f"late#k={k}"):
            if k < ticks:
                tick(1, k)

    begin(0)
    mine = tokw.at[:, span(tp * dl, dl)]
    for d in range(1, TP):
        remote(mine, mine, tok_sem.at[0], tok_sem.at[1], (fs, (tp + d) % TP)).start()
    mine = gainw.at[:, span(tp * dl, dl)]
    for d in range(1, TP):
        remote(mine, mine, gain_sem.at[0], gain_sem.at[1], (fs, (tp + d) % TP)).start()
    for k in range(ticks):
        with jax.named_scope(f"early#k={k}"):
            tick(0, k)
            if k == ticks - 1 - LATE:
                begin(1)
            if k >= ticks - LATE:
                tick(1, k - (ticks - LATE))
    with jax.named_scope("tokens"):
        await_recv(tokw.at[:, pl.ds(0, (TP - 1) * dl)], tok_sem.at[1])
        await_recv(gainw.at[:, pl.ds(0, (TP - 1) * dl)], gain_sem.at[1])

    def taps_of(v, tap_ref, cols):
        at = lax.broadcasted_iota(jnp.int32, v.shape, 0)
        one = jnp.where(at >= 1, pltpu.roll(v, 1, 0), 0.0)
        two = jnp.where(at >= 2, pltpu.roll(v, 2, 0), 0.0)
        return v * tap_ref[2:3, cols] + one * tap_ref[1:2, cols] + two * tap_ref[0:1, cols]

    def seq(s):
        return pl.ds(s * SEQ_LEN, SEQ_LEN)

    def project(left, g, r, target):
        def one(n, carry):
            at = pl.multiple_of(n * 256, 256)
            right = g[:, :, :, :, pl.ds(at, 256)].reshape(D, 256)
            target[r, pl.ds(at, 256)] = jnp.dot(left[r, :], right, preferred_element_type=F32).astype(BF16)
            return carry

        lax.fori_loop(0, target.shape[1] // 256, one, 0)

    def branch_out(slot, s, left, g, first_col, cols, ppart, pown, dbuf):
        def theirs(j, carry):
            right = g[2 * j + 1 - c, :, :, :, first_col : first_col + cols].reshape(dl, cols)
            ppart[s, j] = nt_dot(left[seq(s), :], right).astype(BF16)
            return carry

        lax.fori_loop(0, X, theirs, 0)
        remote(ppart.at[s], dbuf.at[s], dsend.at[slot], drecv.at[slot * n_seq + s], (fs, partner)).start()

        def ours(j, carry):
            right = g[2 * j + c, :, :, :, first_col : first_col + cols].reshape(dl, cols)
            pown[s, j] = nt_dot(left[seq(s), :], right).astype(BF16)
            return carry

        lax.fori_loop(0, X, ours, 0)

    def cross(slot, s, pown, dbuf, sbuf, rbuf):
        await_recv(dbuf.at[s], drecv.at[slot * n_seq + s])
        for d in away:
            j = (x + d) % X
            sbuf[s, d - 1] = (pown[s, j].astype(F32) + dbuf[s, j].astype(F32)).astype(BF16)
            remote(
                sbuf.at[s, d - 1], rbuf.at[s, d - 1], xsend.at[slot], xrecv.at[slot * n_seq + s], (fs, 2 * j + c)
            ).start()

    def total(slot, s, pown, dbuf, rbuf):
        await_recv(rbuf.at[s], xrecv.at[slot * n_seq + s])
        acc = pown[s, x].astype(F32) + dbuf[s, x].astype(F32)
        for d in away:
            acc = acc + rbuf[s, d - 1].astype(F32)
        return acc

    own_cols = span(tp * dl, dl)

    def mixer(s):
        with jax.named_scope(f"mixer#s={s}"):
            project(tokw, g12, seq(s), proj)
            for at in range(0, dl, 128):
                cols = pl.ds(at, 128)
                outer = proj[seq(s), cols].astype(F32)
                inner = proj[seq(s), pl.ds(dl + at, 128)].astype(F32)
                value = proj[seq(s), pl.ds(2 * dl + at, 128)].astype(F32)
                gated[seq(s), cols] = (outer * taps_of(inner * value, mtapf, cols)).astype(BF16)
            branch_out(0, s, gated, g12, 3 * dl, dl, ppart_m, pown_m, dbuf_m)

    def mixer_cross(s):
        with jax.named_scope(f"mcross#s={s}"):
            cross(0, s, pown_m, dbuf_m, sbuf_m, rbuf_m)

    def gather_start(s):
        with jax.named_scope(f"rs#s={s}"):
            branchw[seq(s), own_cols] = total(0, s, pown_m, dbuf_m, rbuf_m).astype(BF16)
            mine = branchw.at[seq(s), own_cols]
            for d in away:
                remote(mine, mine, agx_send, agx_recv.at[s], (fs, 2 * ((x + d) % X) + c)).start()
            remote(mine, mine, agd_send, agd_recv.at[s], (fs, partner)).start()

    def gather_share(s):
        with jax.named_scope(f"agx#s={s}"):
            await_recv(branchw.at[seq(s), pl.ds(0, (X - 1) * dl)], agx_recv.at[s])
            for d in away:
                theirs = branchw.at[seq(s), span((2 * ((x + d) % X) + c) * dl, dl)]
                remote(theirs, theirs, agd_send, agd_recv.at[s], (fs, partner)).start()

    def first_norm(s):
        with jax.named_scope(f"agd#s={s}"):
            await_recv(branchw.at[seq(s), pl.ds(0, X * dl)], agd_recv.at[s])
        with jax.named_scope(f"norm#s={s}"):
            zero = jnp.zeros((SEQ_LEN, 128), F32)

            def summed(k, acc):
                cols = span(k * 128, 128)
                v = residual_scale * tokw[seq(s), cols].astype(F32) + branchw[seq(s), cols].astype(F32)
                normed[:, cols] = v
                return acc + v

            mean = jnp.sum(lax.fori_loop(0, D // 128, summed, zero), axis=1, keepdims=True) * (1.0 / D)

            def squared(k, acc):
                v = normed[:, span(k * 128, 128)] - mean
                return acc + v * v

            spread = jnp.sum(lax.fori_loop(0, D // 128, squared, zero), axis=1, keepdims=True) * (1.0 / D)
            scale = lax.rsqrt(spread + norm_epsilon)

            def scaled(k, carry):
                cols = span(k * 128, 128)
                firstw[seq(s), cols] = ((normed[:, cols] - mean) * scale * gainw[0:1, cols]).astype(BF16)
                return carry

            lax.fori_loop(0, D // 128, scaled, 0)

    def ffn(s):
        with jax.named_scope(f"ffn#s={s}"):
            project(firstw, g34, seq(s), up)
            for at in range(0, fl, 128):
                cols = pl.ds(at, 128)
                left = taps_of(up[seq(s), cols].astype(F32), gtapf, cols)
                right = taps_of(up[seq(s), pl.ds(fl + at, 128)].astype(F32), vtapf, cols)
                hidden[seq(s), cols] = (left / (1.0 + jnp.exp(-left)) * right).astype(BF16)
            branch_out(1, s, hidden, g34, 2 * fl, fl, ppart_f, pown_f, dbuf_f)

    def ffn_cross(s):
        with jax.named_scope(f"fcross#s={s}"):
            cross(1, s, pown_f, dbuf_f, sbuf_f, rbuf_f)

    lane = lax.broadcasted_iota(jnp.int32, (SEQ_LEN, 128), 1)
    line = lax.broadcasted_iota(jnp.int32, (128, SEQ_LEN), 0)

    def last_sums(s):
        with jax.named_scope(f"frs#s={s}"):
            v = residual_scale * firstw[seq(s), own_cols].astype(F32) + total(1, s, pown_f, dbuf_f, rbuf_f)
            ybuf[seq(s), :] = v
            mean = jnp.sum(v, axis=1, keepdims=True) * (1.0 / dl)
            v = v - mean
            square = jnp.sum(v * v, axis=1, keepdims=True)
            both = jnp.where(lane == 0, mean, jnp.where(lane == 1, square, 0.0))
            stats[tp, s] = both.T[:8]
            for d in range(1, TP):
                remote(stats.at[tp, s], stats.at[tp, s], st_send, st_recv.at[s], (fs, (tp + d) % TP)).start()

    def last_norm(s):
        with jax.named_scope(f"final#s={s}"):
            await_recv(stats.at[pl.ds(0, TP - 1), s], st_recv.at[s])
            theirs = stats[:, s]
            means, squares = theirs[:, 0], theirs[:, 1]
            mean = jnp.sum(means, axis=0, keepdims=True) * (1.0 / TP)
            off = means - mean
            spread = jnp.sum(squares, axis=0, keepdims=True) + dl * jnp.sum(off * off, axis=0, keepdims=True)
            scale = lax.rsqrt(spread * (1.0 / D) + norm_epsilon)
            both = jnp.where(line == 0, mean, jnp.where(line == 1, scale, 0.0)).T
            v = (ybuf[seq(s), :] - both[:, 0:1]) * both[:, 1:2]
            out_ref[seq(s), :] = (v * fgain_ref[...].astype(F32).reshape(1, dl)).astype(BF16)

    plan = [(mixer, s) for s in range(n_seq)]
    for s in range(n_seq):
        plan.insert(2 * s + 2, (mixer_cross, s))
    plan += [(gather_start, s) for s in range(n_seq)]
    for s in range(n_seq):
        plan += [(gather_share, s)] + ([(first_norm, s - 1)] if s > 0 else [])
    plan += [(first_norm, n_seq - 1)]
    late = LATE
    for i, (stage, s) in enumerate(plan):
        if LATE_AT[late] == (stage.__name__, s):
            late_tick(late)
            late += 1
        stage(s)
    while late < ticks:
        late_tick(late)
        late += 1
    plan = [(ffn, s) for s in range(n_seq)]
    for s in range(n_seq):
        plan.insert(2 * s + 2, (ffn_cross, s))
    plan += [(last_sums, s) for s in range(n_seq)] + [(last_norm, s) for s in range(n_seq)]
    for stage, s in plan:
        stage(s)

    with jax.named_scope("drain"):
        for w, g in enumerate(groups):
            await_send(g.at[pl.ds(0, Z - 1), 0], wsend.at[2 * w])
            await_send(g.at[:, pl.ds(0, Y - 1)], wsend.at[2 * w + 1])
        await_send(tokw.at[:, pl.ds(0, (TP - 1) * dl)], tok_sem.at[0])
        await_send(gainw.at[:, pl.ds(0, (TP - 1) * dl)], gain_sem.at[0])
        for slot, (ppart, sbuf) in enumerate(((ppart_m, sbuf_m), (ppart_f, sbuf_f))):
            await_send(ppart, dsend.at[slot])
            await_send(sbuf, xsend.at[slot])
        await_send(branchw.at[:, pl.ds(0, (X - 1) * dl)], agx_send)
        await_send(branchw.at[:, pl.ds(0, X * dl)], agd_send)
        await_send(stats.at[pl.ds(0, TP - 1)], st_send)


def layer(cfg, tokens, outer_gate, inner_gate, mix_value, mix_taps, mix_out, mix_gain, ffn_gate, ffn_value, gate_taps, value_taps, ffn_down, ffn_gain):
    Z, Y, TP = cfg
    X = TP // 2
    rows, dl = tokens.shape
    kr = outer_gate.shape[0]
    h = kr // 2
    fl = ffn_gate.shape[1]
    D = TP * dl
    n_seq = rows // SEQ_LEN
    vmem = pl.BlockSpec(memory_space=pltpu.VMEM)
    hbm = pl.BlockSpec(memory_space=pl.ANY)
    dma = pltpu.SemaphoreType.DMA
    exchange = [
        pltpu.VMEM((n_seq, X, SEQ_LEN, dl), BF16),
        pltpu.VMEM((n_seq, X, SEQ_LEN, dl), BF16),
        pltpu.VMEM((n_seq, X, SEQ_LEN, dl), BF16),
        pltpu.VMEM((n_seq, X - 1, SEQ_LEN, dl), BF16),
        pltpu.VMEM((n_seq, X - 1, SEQ_LEN, dl), BF16),
    ]
    return pl.pallas_call(
        functools.partial(kernel, cfg),
        out_shape=jax.ShapeDtypeStruct((rows, dl), BF16),
        in_specs=[hbm, hbm, hbm, hbm, vmem, hbm, vmem, hbm, hbm, vmem, vmem, hbm, vmem],
        out_specs=vmem,
        scratch_shapes=[
            pltpu.VMEM((Z, Y, 2, h, 4 * dl), BF16),
            pltpu.VMEM((Z, Y, 2, h, 3 * fl), BF16),
            pltpu.VMEM((rows, D), BF16),
            pltpu.VMEM((8, D), F32),
            pltpu.VMEM((rows, D), BF16),
            pltpu.VMEM((rows, D), BF16),
            pltpu.VMEM((SEQ_LEN, D), F32),
            pltpu.VMEM((rows, 3 * dl), BF16),
            pltpu.VMEM((rows, dl), BF16),
            pltpu.VMEM((rows, 2 * fl), BF16),
            pltpu.VMEM((rows, fl), BF16),
            *exchange,
            *exchange,
            pltpu.VMEM((rows, dl), F32),
            pltpu.VMEM((TP, n_seq, 8, SEQ_LEN), F32),
            pltpu.VMEM((3, dl), F32),
            pltpu.VMEM((3, fl), F32),
            pltpu.VMEM((3, fl), F32),
            dma((96,)),
            dma((4,)),
            dma((3,)),
            dma((2,)),
            dma((2,)),
            dma((2,)),
            dma((2 * n_seq,)),
            dma((2,)),
            dma((2 * n_seq,)),
            dma,
            dma((n_seq,)),
            dma,
            dma((n_seq,)),
            dma,
            dma((n_seq,)),
        ],
        compiler_params=pltpu.CompilerParams(
            collective_id=0, has_side_effects=True, vmem_limit_bytes=VMEM_LIMIT
        ),
    )(
        tokens,
        outer_gate,
        inner_gate,
        mix_value,
        mix_taps,
        mix_out.T,
        mix_gain,
        ffn_gate,
        ffn_value,
        gate_taps,
        value_taps,
        ffn_down.T,
        ffn_gain,
    )


def solution(mesh):
    placed = (
        P("fs", "tp"),
        P("fs", "tp"),
        P("fs", "tp"),
        P("fs", "tp"),
        P(None, "tp"),
        P("tp", "fs"),
        P("tp"),
        P("fs", "tp"),
        P("fs", "tp"),
        P(None, "tp"),
        P(None, "tp"),
        P("tp", "fs"),
        P("tp"),
    )
    cfg = (RING_Z, RING_Y, mesh.shape["tp"])
    return jax.shard_map(
        functools.partial(layer, cfg), mesh=mesh, in_specs=placed, out_specs=P("fs", "tp"), check_vma=False
    )
```

time: 326 us -> 103 us (0.32)
  waiting for transfers between devices: 192 us -> 0 us
  Pallas kernels: 0 us -> 102 us
  blocking collectives: 59.4 us -> 0 us
  starting transfers between devices: 34.1 us -> 0 us
  matrix products: 13.4 us -> 0 us
  between operations: 13.4 us -> 0.01 us
  local copies, waits for them, and re-layouts: 7.32 us -> 1.62 us
  other arithmetic: 4.73 us -> 0 us
    all_gather x3 -> x0, waiting for transfers between devices: 162 us -> none  [the longest x2 84.2 us: in_one_piece(): lax.all_gather(both, axis, axis=dim, tiled=True)]
    pallas_call x0 -> x1, Pallas kernels: none -> 102 us  [layer(): pl.pallas_call(functools.partial(kernel, cfg), out_shape=jax.ShapeDtypeSt...]
    all_to_all x2 -> x0, blocking collectives: 59.4 us -> none  [the longest x1 29.8 us: copy_for_each(): return lax.all_to_all(copies, axis, split_axis=0, concat_axis=0, tiled=True)]
    all_to_all x5 -> x0, starting transfers between devices: 34.1 us -> none  [the longest x4 25.5 us: copy_for_each(): return lax.all_to_all(copies, axis, split_axis=0, concat_axis=0, tiled=True)]
    all_to_all x5 -> x0, waiting for transfers between devices: 29.2 us -> none  [the longest x1 19.8 us: sent_and_summed(): blocks = lax.all_to_all(split_up(value, dim, peers), axis, 0, 0, tiled=True)]
    dot_general x7 -> x0, matrix products: 13.4 us -> none  [the longest x3 5.89 us: fold_rows(): jnp.dot(whole, piece, preferred_element_type=jnp.float32)]
    broadcast_in_dim x5 -> x0, local copies, waits for them, and re-layouts: 3.83 us -> none  [copy_for_each(): copies = jnp.broadcast_to(value, (lax.axis_size(axis), *value.shape))]
  transfers between devices with their start and end apart: 8 -> 0, of which waited for: 6 -> 0; matrix products, arithmetic and copies ran while one was open for 6% -> 0% of each run, Pallas kernels for 0% -> 0%
where the time goes in v2:
time: 103 us
  Pallas kernels  102 us (99%)
  local copies, waits for them, and re-layouts  1.62 us (2%)
    pallas_call x1, Pallas kernels, layer(): pl.pallas_call(functools.partial(kernel, cfg), out_shape=jax.ShapeDtypeSt...  102 us

profile of v2, /device:TPU:1, one launch (start us, length us, event | category | flops | bytes accessed | tf_op | source)
XLA Modules:
  0.0 103.2 jit_solution(13572299707800330022)
XLA Ops:
  0.0 101.6 %shard_map.127 = bf16[384,256]{1,0:T(8,128)(2,1)} custom-call(bf16[384,256]{1,0:T(8,128)(2,1)} %tok_ref.1, bf16[32,256]{1,0:T(8,128)(2,1)} %og_ref.1, bf16[32,256]{1,0:T(8,128)(2,1)} %ig_ref.1, bf16[32,256]{1,0:T(8,128)(2,1)} %mv_ref.1, bf16[3,256]{1,0:T(4,128)(2,1)} %mtaps_ref.1, bf16[32,256]{1,0:T(8,128)(2,1)} %bitcast.3, bf16[256]{0:T(256)(128)(2,1)} %mgain_ref.1, ...), custom_call_target="tpu_custom_call" | custom-call | tf_op jit(solution)/shard_map/pallas_call | solution.py:466
  101.6 1.6 %copy.15 = bf16[384,256]{1,0:T(8,128)(2,1)} copy(bf16[384,256]{1,0:T(8,128)(2,1)} %shard_map.127) | data formatting | bytes 393216

commit v3 on v2

--- a/solution.py
+++ b/solution.py
@@ -14,23 +14,17 @@
 norm_epsilon = 1e-05
 MESH = pl.DeviceIdType.MESH
 RIGHT, LEFT = 0, 1
-LATE = 2
+W34_FIRST = 0
+W34_SECOND = (5, 5, 6, 6, 6)
 LATE_AT = {
-    2: ("mixer", 2),
-    3: ("gather_start", 0),
-    4: ("gather_start", 1),
-    5: ("gather_share", 0),
-    6: ("gather_share", 1),
-    7: ("gather_share", 2),
-    8: None,
+    1: ("mixer_cross", 2),
+    2: ("gather_start", 1),
+    3: ("gather_share", 0),
+    4: ("gather_share", 1),
 }
 VMEM_LIMIT = 60 * 1024 * 1024
 F32 = jnp.float32
 BF16 = jnp.bfloat16
-
-
-def nt_dot(a, b):
-    return lax.dot_general(a, b, (((1,), (1,)), ((), ())), preferred_element_type=F32)
 
 
 def kernel(
@@ -56,6 +50,7 @@
     branchw,
     firstw,
     normed,
+    psum,
     proj,
     gated,
     up,
@@ -128,7 +123,7 @@
 
     barrier = pltpu.get_barrier_semaphore()
     for axis in ("y", "z"):
-        for step in (1, -1):
+        for step in (1, -1, 2, -2):
             pl.semaphore_signal(barrier, inc=1, device_id=ring_id(axis, step), device_id_type=MESH)
     for d in range(1, TP):
         pl.semaphore_signal(barrier, inc=1, device_id=(fs, (tp + d) % TP), device_id_type=MESH)
@@ -155,7 +150,7 @@
         pltpu.make_async_copy(g.at[z, y], g.at[z, y], loc_sem.at[i]).wait()
     own_tokens.wait()
     with jax.named_scope("greet"):
-        pl.semaphore_wait(barrier, 4 + TP - 1)
+        pl.semaphore_wait(barrier, 8 + TP - 1)
 
     def piece(w, colour, one, two):
         return groups[w].at[two, one, 0] if colour == 0 else groups[w].at[one, two, 1]
@@ -171,10 +166,12 @@
         for way in (RIGHT, LEFT):
             if step == n // 2 - 1 and way != w % 2:
                 continue
-            origin = (me - step + n) % n if way == RIGHT else (me + step) % n
+            straight = w == 0 and step == 1 and n >= 8
+            reach, back = (2, 0) if straight else (1, step)
+            origin = (me - back + n) % n if way == RIGHT else (me + back) % n
             ref = piece(w, colour, origin, other)
             remote(
-                ref, ref, wsend.at[2 * w], recv_sem(w, colour, 5, step), ring_id(axis, 1 if way == RIGHT else -1)
+                ref, ref, wsend.at[2 * w], recv_sem(w, colour, 5, step), ring_id(axis, reach if way == RIGHT else -reach)
             ).start()
 
     def first_count(colour, step):
@@ -207,53 +204,100 @@
         g = groups[w]
         await_recv(g.at[0, 0, 0] if count == 1 else g.at[pl.ds(0, count), 0, 0], sem)
 
-    def begin(w):
-        for colour in range(2):
-            send_first(w, colour, 0)
-        for colour in range(2):
-            send_second(w, colour, 0, 0)
-
-    def tick(w, k):
+    def first_arrives(w, k):
         for colour in range(2):
             n1 = rings(colour)[0][1]
-            if 0 <= k < n1 // 2:
+            if k < n1 // 2:
                 await_pieces(w, first_count(colour, k), recv_sem(w, colour, 5, k))
-                if k + 1 < n1 // 2:
+                if k + 1 < n1 // 2 and (w == 1 or k > 0 or n1 < 8):
                     send_first(w, colour, k + 1)
-                send_second(w, colour, k + 1, 0)
-        for step in range(max(Y, Z) // 2):
-            for colour in range(2):
-                n1, n2 = rings(colour)[0][1], rings(colour)[1][1]
-                g = k - step
-                if 0 <= g <= n1 // 2 and step < n2 // 2:
-                    await_pieces(w, second_count(colour, g, step), recv_sem(w, colour, g, step))
-                    if step + 1 < n2 // 2:
-                        send_second(w, colour, g, step + 1)
-
-    ticks = (Y + Z) // 2
+
+    def second_begins(w, g):
+        for colour in range(2):
+            if g <= rings(colour)[0][1] // 2:
+                send_second(w, colour, g, 0)
+
+    def second_arrives(w, g, step):
+        for colour in range(2):
+            n1, n2 = rings(colour)[0][1], rings(colour)[1][1]
+            if g <= n1 // 2 and step < n2 // 2:
+                await_pieces(w, second_count(colour, g, step), recv_sem(w, colour, g, step))
+                if step + 1 < n2 // 2:
+                    send_second(w, colour, g, step + 1)
+
+    most = max(Y, Z) // 2
+    first_tick = {(0, k): max(0, k - 1) if most >= 4 else k for k in range(most)}
+    first_tick.update({(1, k): W34_FIRST + 1 + k for k in range(most)})
+    second_tick = {(0, g): first_tick[0, g - 1] if g > 0 else -1 for g in range(most + 1)}
+    for g in range(most + 1):
+        second_tick[1, g] = max(W34_SECOND[min(g, 4)], first_tick[1, g - 1] if g > 0 else 0)
+    ready = max(second_tick[0, g] for g in range(most + 1)) + most
+    ticks = max(second_tick[1, g] for g in range(most + 1)) + most
+
+    def tick(at):
+        for w in range(2):
+            firsts = [k for k in range(most) if first_tick[w, k] == at]
+            for k in firsts[:1]:
+                first_arrives(w, k)
+                if w == 0:
+                    second_begins(w, k + 1)
+            for step in range(most):
+                for g in range(most + 1):
+                    if second_tick[w, g] + 1 + step == at:
+                        second_arrives(w, g, step)
+            for k in firsts[1:]:
+                first_arrives(w, k)
+                if w == 0:
+                    second_begins(w, k + 1)
+            if w == 1:
+                if at == W34_FIRST:
+                    for colour in range(2):
+                        send_first(1, colour, 0)
+                for g in range(most + 1):
+                    if second_tick[1, g] == at:
+                        second_begins(1, g)
 
     def late_tick(k):
         with jax.named_scope(f"late#k={k}"):
-            if k < ticks:
-                tick(1, k)
-
-    begin(0)
+            tick(k)
+
+    for colour in range(2):
+        send_first(0, colour, 0)
+    second_begins(0, 0)
+    for colour in range(2):
+        if rings(colour)[0][1] >= 8:
+            send_first(0, colour, 1)
     mine = tokw.at[:, span(tp * dl, dl)]
     for d in range(1, TP):
         remote(mine, mine, tok_sem.at[0], tok_sem.at[1], (fs, (tp + d) % TP)).start()
     mine = gainw.at[:, span(tp * dl, dl)]
     for d in range(1, TP):
         remote(mine, mine, gain_sem.at[0], gain_sem.at[1], (fs, (tp + d) % TP)).start()
-    for k in range(ticks):
+    for k in range(ready):
         with jax.named_scope(f"early#k={k}"):
-            tick(0, k)
-            if k == ticks - 1 - LATE:
-                begin(1)
-            if k >= ticks - LATE:
-                tick(1, k - (ticks - LATE))
+            tick(k)
     with jax.named_scope("tokens"):
         await_recv(tokw.at[:, pl.ds(0, (TP - 1) * dl)], tok_sem.at[1])
         await_recv(gainw.at[:, pl.ds(0, (TP - 1) * dl)], gain_sem.at[1])
+
+    deep = D // Z
+
+    def plane_dot(plane, at):
+        right = g12[plane, :, :, :, pl.ds(at, 256)].reshape(deep, 256)
+        return jnp.dot(tokw[:, span(plane * deep, deep)], right, preferred_element_type=F32)
+
+    with jax.named_scope("planes"):
+        for at in range(0, 3 * dl, 256):
+            psum[:, at : at + 256] = plane_dot((z + Z // 2 + 1) % Z, at)
+
+        def add_plane(i, carry):
+            for at in range(0, 3 * dl, 256):
+                psum[:, at : at + 256] += plane_dot((z + Z // 2 + i) % Z, at)
+            return carry
+
+        lax.fori_loop(2, Z, add_plane, 0)
+    with jax.named_scope(f"early#k={ready}"):
+        tick(ready)
 
     def taps_of(v, tap_ref, cols):
         at = lax.broadcasted_iota(jnp.int32, v.shape, 0)
@@ -273,21 +317,21 @@
 
         lax.fori_loop(0, target.shape[1] // 256, one, 0)
 
-    def branch_out(slot, s, left, g, first_col, cols, ppart, pown, dbuf):
+    def branch_out(slot, s, turned, g, first_col, cols, ppart, pown, dbuf):
         def theirs(j, carry):
-            right = g[2 * j + 1 - c, :, :, :, first_col : first_col + cols].reshape(dl, cols)
-            ppart[s, j] = nt_dot(left[seq(s), :], right).astype(BF16)
+            left = g[2 * j + 1 - c, :, :, :, first_col : first_col + cols].reshape(dl, cols)
+            ppart[s, j] = jnp.dot(left, turned[s], preferred_element_type=F32).astype(BF16)
             return carry
 
-        lax.fori_loop(0, X, theirs, 0)
+        lax.fori_loop(0, X, theirs, 0, unroll=True)
         remote(ppart.at[s], dbuf.at[s], dsend.at[slot], drecv.at[slot * n_seq + s], (fs, partner)).start()
 
         def ours(j, carry):
-            right = g[2 * j + c, :, :, :, first_col : first_col + cols].reshape(dl, cols)
-            pown[s, j] = nt_dot(left[seq(s), :], right).astype(BF16)
+            left = g[2 * j + c, :, :, :, first_col : first_col + cols].reshape(dl, cols)
+            pown[s, j] = jnp.dot(left, turned[s], preferred_element_type=F32).astype(BF16)
             return carry
 
-        lax.fori_loop(0, X, ours, 0)
+        lax.fori_loop(0, X, ours, 0, unroll=True)
 
     def cross(slot, s, pown, dbuf, sbuf, rbuf):
         await_recv(dbuf.at[s], drecv.at[slot * n_seq + s])
@@ -303,19 +347,22 @@
         acc = pown[s, x].astype(F32) + dbuf[s, x].astype(F32)
         for d in away:
             acc = acc + rbuf[s, d - 1].astype(F32)
-        return acc
+        return acc.T
 
     own_cols = span(tp * dl, dl)
 
     def mixer(s):
         with jax.named_scope(f"mixer#s={s}"):
-            project(tokw, g12, seq(s), proj)
+            if s == 0:
+                for at in range(0, 3 * dl, 256):
+                    last = psum[:, at : at + 256] + plane_dot((z + Z // 2) % Z, at)
+                    proj[:, at : at + 256] = last.astype(BF16)
             for at in range(0, dl, 128):
                 cols = pl.ds(at, 128)
                 outer = proj[seq(s), cols].astype(F32)
                 inner = proj[seq(s), pl.ds(dl + at, 128)].astype(F32)
                 value = proj[seq(s), pl.ds(2 * dl + at, 128)].astype(F32)
-                gated[seq(s), cols] = (outer * taps_of(inner * value, mtapf, cols)).astype(BF16)
+                gated[s, cols, :] = (outer * taps_of(inner * value, mtapf, cols)).T.astype(BF16)
             branch_out(0, s, gated, g12, 3 * dl, dl, ppart_m, pown_m, dbuf_m)
 
     def mixer_cross(s):
@@ -349,13 +396,13 @@
                 normed[:, cols] = v
                 return acc + v
 
-            mean = jnp.sum(lax.fori_loop(0, D // 128, summed, zero), axis=1, keepdims=True) * (1.0 / D)
+            mean = jnp.sum(lax.fori_loop(0, D // 128, summed, zero, unroll=4), axis=1, keepdims=True) * (1.0 / D)
 
             def squared(k, acc):
                 v = normed[:, span(k * 128, 128)] - mean
                 return acc + v * v
 
-            spread = jnp.sum(lax.fori_loop(0, D // 128, squared, zero), axis=1, keepdims=True) * (1.0 / D)
+            spread = jnp.sum(lax.fori_loop(0, D // 128, squared, zero, unroll=4), axis=1, keepdims=True) * (1.0 / D)
             scale = lax.rsqrt(spread + norm_epsilon)
 
             def scaled(k, carry):
@@ -363,7 +410,7 @@
                 firstw[seq(s), cols] = ((normed[:, cols] - mean) * scale * gainw[0:1, cols]).astype(BF16)
                 return carry
 
-            lax.fori_loop(0, D // 128, scaled, 0)
+            lax.fori_loop(0, D // 128, scaled, 0, unroll=4)
 
     def ffn(s):
         with jax.named_scope(f"ffn#s={s}"):
@@ -372,7 +419,7 @@
                 cols = pl.ds(at, 128)
                 left = taps_of(up[seq(s), cols].astype(F32), gtapf, cols)
                 right = taps_of(up[seq(s), pl.ds(fl + at, 128)].astype(F32), vtapf, cols)
-                hidden[seq(s), cols] = (left / (1.0 + jnp.exp(-left)) * right).astype(BF16)
+                hidden[s, cols, :] = (left / (1.0 + jnp.exp(-left)) * right).T.astype(BF16)
             branch_out(1, s, hidden, g34, 2 * fl, fl, ppart_f, pown_f, dbuf_f)
 
     def ffn_cross(s):
@@ -410,24 +457,18 @@
     plan = [(mixer, s) for s in range(n_seq)]
     for s in range(n_seq):
         plan.insert(2 * s + 2, (mixer_cross, s))
-    plan += [(gather_start, s) for s in range(n_seq)]
+    plan += [(gather_start, s) for s in range(n_seq)] + [(gather_share, s) for s in range(n_seq)]
     for s in range(n_seq):
-        plan += [(gather_share, s)] + ([(first_norm, s - 1)] if s > 0 else [])
-    plan += [(first_norm, n_seq - 1)]
-    late = LATE
-    for i, (stage, s) in enumerate(plan):
-        if LATE_AT[late] == (stage.__name__, s):
+        plan += [(first_norm, s)] + ([(ffn_cross, s - 1)] if s > 0 else []) + [(ffn, s)]
+    plan += [(ffn_cross, n_seq - 1)]
+    share = plan.index((gather_share, n_seq - 1))
+    plan.insert(min(share + 2, len(plan)), plan.pop(share))
+    late = ready + 1
+    plan += [(last_sums, s) for s in range(n_seq)] + [(last_norm, s) for s in range(n_seq)]
+    for stage, s in plan:
+        while late <= ticks and (LATE_AT.get(late - ready) == (stage.__name__, s) or stage is first_norm):
             late_tick(late)
             late += 1
-        stage(s)
-    while late < ticks:
-        late_tick(late)
-        late += 1
-    plan = [(ffn, s) for s in range(n_seq)]
-    for s in range(n_seq):
-        plan.insert(2 * s + 2, (ffn_cross, s))
-    plan += [(last_sums, s) for s in range(n_seq)] + [(last_norm, s) for s in range(n_seq)]
-    for stage, s in plan:
         stage(s)
 
     with jax.named_scope("drain"):
@@ -457,11 +498,11 @@
     hbm = pl.BlockSpec(memory_space=pl.ANY)
     dma = pltpu.SemaphoreType.DMA
     exchange = [
-        pltpu.VMEM((n_seq, X, SEQ_LEN, dl), BF16),
-        pltpu.VMEM((n_seq, X, SEQ_LEN, dl), BF16),
-        pltpu.VMEM((n_seq, X, SEQ_LEN, dl), BF16),
-        pltpu.VMEM((n_seq, X - 1, SEQ_LEN, dl), BF16),
-        pltpu.VMEM((n_seq, X - 1, SEQ_LEN, dl), BF16),
+        pltpu.VMEM((n_seq, X, dl, SEQ_LEN), BF16),
+        pltpu.VMEM((n_seq, X, dl, SEQ_LEN), BF16),
+        pltpu.VMEM((n_seq, X, dl, SEQ_LEN), BF16),
+        pltpu.VMEM((n_seq, X - 1, dl, SEQ_LEN), BF16),
+        pltpu.VMEM((n_seq, X - 1, dl, SEQ_LEN), BF16),
     ]
     return pl.pallas_call(
         functools.partial(kernel, cfg),
@@ -476,10 +517,11 @@
             pltpu.VMEM((rows, D), BF16),
             pltpu.VMEM((rows, D), BF16),
             pltpu.VMEM((SEQ_LEN, D), F32),
+            pltpu.VMEM((rows, 3 * dl), F32),
             pltpu.VMEM((rows, 3 * dl), BF16),
-            pltpu.VMEM((rows, dl), BF16),
+            pltpu.VMEM((n_seq, dl, SEQ_LEN), BF16),
             pltpu.VMEM((rows, 2 * fl), BF16),
-            pltpu.VMEM((rows, fl), BF16),
+            pltpu.VMEM((n_seq, fl, SEQ_LEN), BF16),
             *exchange,
             *exchange,
             pltpu.VMEM((rows, dl), F32),

time: 103 us -> 95.4 us (0.926)
  Pallas kernels: 102 us -> 93.6 us
    pallas_call x1, Pallas kernels: 102 us -> 93.6 us  [layer(): pl.pallas_call(functools.partial(kernel, cfg), out_shape=jax.ShapeDtypeSt...]
where the time goes in v3:
time: 95.4 us; the launch traced here: 95.2 us
  Pallas kernels  93.6 us (98%)
  local copies, waits for them, and re-layouts  1.62 us (2%)
    pallas_call x1, Pallas kernels, layer(): pl.pallas_call(functools.partial(kernel, cfg), out_shape=jax.ShapeDtypeSt...  93.6 us

profile of v3, /device:TPU:1, one launch (start us, length us, event | category | flops | bytes accessed | tf_op | source)
XLA Modules:
  0.0 95.2 jit_solution(9770954878191893433)
XLA Ops:
  0.0 93.6 %shard_map.127 = bf16[384,256]{1,0:T(8,128)(2,1)} custom-call(bf16[384,256]{1,0:T(8,128)(2,1)} %tok_ref.1, bf16[32,256]{1,0:T(8,128)(2,1)} %og_ref.1, bf16[32,256]{1,0:T(8,128)(2,1)} %ig_ref.1, bf16[32,256]{1,0:T(8,128)(2,1)} %mv_ref.1, bf16[3,256]{1,0:T(4,128)(2,1)} %mtaps_ref.1, bf16[32,256]{1,0:T(8,128)(2,1)} %bitcast.3, bf16[256]{0:T(256)(128)(2,1)} %mgain_ref.1, ...), custom_call_target="tpu_custom_call" | custom-call | tf_op jit(solution)/shard_map/pallas_call | solution.py:507
  93.6 1.6 %copy.15 = bf16[384,256]{1,0:T(8,128)(2,1)} copy(bf16[384,256]{1,0:T(8,128)(2,1)} %shard_map.127) | data formatting | bytes 393216

commit v4 on v3

--- a/solution.py
+++ b/solution.py
@@ -15,9 +15,9 @@
 MESH = pl.DeviceIdType.MESH
 RIGHT, LEFT = 0, 1
 W34_FIRST = 0
-W34_SECOND = (5, 5, 6, 6, 6)
+W34_SECOND = (6, 6, 6, 6, 6)
 LATE_AT = {
-    1: ("mixer_cross", 2),
+    1: ("gather_start", 0),
     2: ("gather_start", 1),
     3: ("gather_share", 0),
     4: ("gather_share", 1),
@@ -146,9 +146,11 @@
     mtapf[...] = mtaps_ref[...].astype(F32)
     gtapf[...] = gtaps_ref[...].astype(F32)
     vtapf[...] = vtaps_ref[...].astype(F32)
-    for i, g in enumerate(groups):
-        pltpu.make_async_copy(g.at[z, y], g.at[z, y], loc_sem.at[i]).wait()
-    own_tokens.wait()
+
+    def placed(w):
+        pltpu.make_async_copy(groups[w].at[z, y], groups[w].at[z, y], loc_sem.at[w]).wait()
+
+    placed(0)
     with jax.named_scope("greet"):
         pl.semaphore_wait(barrier, 8 + TP - 1)
 
@@ -251,6 +253,7 @@
                     second_begins(w, k + 1)
             if w == 1:
                 if at == W34_FIRST:
+                    placed(1)
                     for colour in range(2):
                         send_first(1, colour, 0)
                 for g in range(most + 1):
@@ -267,6 +270,7 @@
     for colour in range(2):
         if rings(colour)[0][1] >= 8:
             send_first(0, colour, 1)
+    own_tokens.wait()
     mine = tokw.at[:, span(tp * dl, dl)]
     for d in range(1, TP):
         remote(mine, mine, tok_sem.at[0], tok_sem.at[1], (fs, (tp + d) % TP)).start()
@@ -454,19 +458,17 @@
             v = (ybuf[seq(s), :] - both[:, 0:1]) * both[:, 1:2]
             out_ref[seq(s), :] = (v * fgain_ref[...].astype(F32).reshape(1, dl)).astype(BF16)
 
-    plan = [(mixer, s) for s in range(n_seq)]
-    for s in range(n_seq):
-        plan.insert(2 * s + 2, (mixer_cross, s))
-    plan += [(gather_start, s) for s in range(n_seq)] + [(gather_share, s) for s in range(n_seq)]
-    for s in range(n_seq):
-        plan += [(first_norm, s)] + ([(ffn_cross, s - 1)] if s > 0 else []) + [(ffn, s)]
+    plan = [(mixer, s) for s in range(n_seq)] + [(mixer_cross, s) for s in range(n_seq)]
+    plan += [(gather_start, s) for s in range(n_seq)] + [(gather_share, 0), (first_norm, 0)]
+    plan += [(gather_share, s) for s in range(1, n_seq)][:1] + [(ffn, 0)]
+    plan += [(gather_share, s) for s in range(2, n_seq)]
+    for s in range(1, n_seq):
+        plan += [(first_norm, s), (ffn_cross, s - 1), (ffn, s)]
     plan += [(ffn_cross, n_seq - 1)]
-    share = plan.index((gather_share, n_seq - 1))
-    plan.insert(min(share + 2, len(plan)), plan.pop(share))
     late = ready + 1
     plan += [(last_sums, s) for s in range(n_seq)] + [(last_norm, s) for s in range(n_seq)]
     for stage, s in plan:
-        while late <= ticks and (LATE_AT.get(late - ready) == (stage.__name__, s) or stage is first_norm):
+        while late <= ticks and (LATE_AT.get(late - ready) == (stage.__name__, s) or stage is ffn):
             late_tick(late)
             late += 1
         stage(s)
@@ -506,7 +508,7 @@
     ]
     return pl.pallas_call(
         functools.partial(kernel, cfg),
-        out_shape=jax.ShapeDtypeStruct((rows, dl), BF16),
+        out_shape=pltpu.VMEM((rows, dl), BF16),
         in_specs=[hbm, hbm, hbm, hbm, vmem, hbm, vmem, hbm, hbm, vmem, vmem, hbm, vmem],
         out_specs=vmem,
         scratch_shapes=[

time: 95.4 us -> 91.6 us (0.960)
  Pallas kernels: 93.6 us -> 90.8 us
    pallas_call x1, Pallas kernels: 93.6 us -> 90.8 us  [layer(): pl.pallas_call(functools.partial(kernel, cfg), out_shape=pltpu.VMEM((rows...]
where the time goes in v4:
time: 91.6 us; the launch traced here: 91.5 us
  Pallas kernels  90.8 us (99%)
    pallas_call x1, Pallas kernels, layer(): pl.pallas_call(functools.partial(kernel, cfg), out_shape=pltpu.VMEM((rows...  90.8 us

profile of v4, /device:TPU:1, one launch (start us, length us, event | category | flops | bytes accessed | tf_op | source)
XLA Modules:
  0.0 91.5 jit_solution(11996326624335171759)
XLA Ops:
  0.0 90.8 %shard_map.127 = bf16[384,256]{1,0:T(8,128)(2,1)S(1)} custom-call(bf16[384,256]{1,0:T(8,128)(2,1)} %tok_ref.1, bf16[32,256]{1,0:T(8,128)(2,1)} %og_ref.1, bf16[32,256]{1,0:T(8,128)(2,1)} %ig_ref.1, bf16[32,256]{1,0:T(8,128)(2,1)} %mv_ref.1, bf16[3,256]{1,0:T(4,128)(2,1)} %mtaps_ref.1, bf16[32,256]{1,0:T(8,128)(2,1)} %bitcast.3, bf16[256]{0:T(256)(128)(2,1)} %mgain_ref.1, ...), custom_call_target="tpu_custom_call" | custom-call | tf_op jit(solution)/shard_map/pallas_call | solution.py:509
  90.8 0.7 copy.15

commit v5 on v4

--- a/solution.py
+++ b/solution.py
@@ -15,8 +15,10 @@
 MESH = pl.DeviceIdType.MESH
 RIGHT, LEFT = 0, 1
 W34_FIRST = 0
-W34_SECOND = (6, 6, 6, 6, 6)
+W34_BEGIN = 5
+W34_SECOND = (5, 5, 6, 6, 6)
 LATE_AT = {
+    0: ("mixer_cross", 0),
     1: ("gather_start", 0),
     2: ("gather_start", 1),
     3: ("gather_share", 0),
@@ -233,11 +235,14 @@
     second_tick = {(0, g): first_tick[0, g - 1] if g > 0 else -1 for g in range(most + 1)}
     for g in range(most + 1):
         second_tick[1, g] = max(W34_SECOND[min(g, 4)], first_tick[1, g - 1] if g > 0 else 0)
+    begin_tick = {g: max(W34_BEGIN, first_tick[1, g - 1] if g > 0 else 0) for g in range(most + 1)}
+    for g in range(most + 1):
+        second_tick[1, g] = max(second_tick[1, g], begin_tick[g])
     ready = max(second_tick[0, g] for g in range(most + 1)) + most
     ticks = max(second_tick[1, g] for g in range(most + 1)) + most
 
-    def tick(at):
-        for w in range(2):
+    def tick(at, which=(0, 1)):
+        for w in which:
             firsts = [k for k in range(most) if first_tick[w, k] == at]
             for k in firsts[:1]:
                 first_arrives(w, k)
@@ -257,12 +262,12 @@
                     for colour in range(2):
                         send_first(1, colour, 0)
                 for g in range(most + 1):
-                    if second_tick[1, g] == at:
+                    if begin_tick[g] == at:
                         second_begins(1, g)
 
     def late_tick(k):
         with jax.named_scope(f"late#k={k}"):
-            tick(k)
+            tick(k, (1,))
 
     for colour in range(2):
         send_first(0, colour, 0)
@@ -301,7 +306,7 @@
 
         lax.fori_loop(2, Z, add_plane, 0)
     with jax.named_scope(f"early#k={ready}"):
-        tick(ready)
+        tick(ready, (0,))
 
     def taps_of(v, tap_ref, cols):
         at = lax.broadcasted_iota(jnp.int32, v.shape, 0)
@@ -465,7 +470,7 @@
     for s in range(1, n_seq):
         plan += [(first_norm, s), (ffn_cross, s - 1), (ffn, s)]
     plan += [(ffn_cross, n_seq - 1)]
-    late = ready + 1
+    late = ready
     plan += [(last_sums, s) for s in range(n_seq)] + [(last_norm, s) for s in range(n_seq)]
     for stage, s in plan:
         while late <= ticks and (LATE_AT.get(late - ready) == (stage.__name__, s) or stage is ffn):

time: 91.6 us -> 90.3 us (0.986)
  Pallas kernels: 90.8 us -> 89.4 us
    pallas_call x1, Pallas kernels: 90.8 us -> 89.4 us  [layer(): pl.pallas_call(functools.partial(kernel, cfg), out_shape=pltpu.VMEM((rows...]
where the time goes in v5:
time: 90.3 us; the launch traced here: 90.1 us
  Pallas kernels  89.4 us (99%)
    pallas_call x1, Pallas kernels, layer(): pl.pallas_call(functools.partial(kernel, cfg), out_shape=pltpu.VMEM((rows...  89.4 us

profile of v5, /device:TPU:1, one launch (start us, length us, event | category | flops | bytes accessed | tf_op | source)
XLA Modules:
  0.0 90.1 jit_solution(1576452873226383035)
XLA Ops:
  0.0 89.4 %shard_map.127 = bf16[384,256]{1,0:T(8,128)(2,1)S(1)} custom-call(bf16[384,256]{1,0:T(8,128)(2,1)} %tok_ref.1, bf16[32,256]{1,0:T(8,128)(2,1)} %og_ref.1, bf16[32,256]{1,0:T(8,128)(2,1)} %ig_ref.1, bf16[32,256]{1,0:T(8,128)(2,1)} %mv_ref.1, bf16[3,256]{1,0:T(4,128)(2,1)} %mtaps_ref.1, bf16[32,256]{1,0:T(8,128)(2,1)} %bitcast.3, bf16[256]{0:T(256)(128)(2,1)} %mgain_ref.1, ...), custom_call_target="tpu_custom_call" | custom-call | tf_op jit(solution)/shard_map/pallas_call | solution.py:514
  89.4 0.7 copy.15
